TPU v7x, 32 devices: a whole 2x2x4 slice. The times are simulated.
32 devices in a mesh: sp: 16 (over z, y, x), tp: 2 (over core).
Axes of the slice: x: 2, y: 2, z: 4, core: 2. Of those that a mesh axis runs over, the one named last changes fastest.
Arguments:
- hidden: bfloat16 [4096, 2048], P('sp', 'tp'), may hold values from -16 to 16
- query_weight: bfloat16 [2048, 1024], P(None, 'tp'), may hold values from -0.125 to 0.125
- key_weight: bfloat16 [2048, 512], P(None, 'tp'), may hold values from -0.125 to 0.125
- value_weight: bfloat16 [2048, 512], P(None, 'tp'), may hold values from -0.125 to 0.125
- head_gate_weight: bfloat16 [2048, 1024], P(None, 'tp'), may hold values from -0.125 to 0.125
- state_in_weight: bfloat16 [2048, 1024], P(None, 'tp'), may hold values from -0.125 to 0.125
- state_gate_weight: bfloat16 [2048, 1024], P(None, 'tp'), may hold values from -0.125 to 0.125
- sink_logit: float32 [16], P('tp'), may hold values from 1 to 6
- decay_real: float32 [64, 64], P('tp'), may hold values from -0.7 to -0.0049
- decay_frequency: float32 [64, 64], P('tp'), may hold values from 0 to 192
- log_step: float32 [64], P('tp'), may hold values from -20 to 0
- input_real: float32 [64, 64, 16], P('tp'), may hold values from -1028 to 1028
- input_imaginary: float32 [64, 64, 16], P('tp'), may hold values from -1028 to 1028
- output_real: float32 [64, 16, 64], P('tp'), may hold values from -0.5 to 0.5
- output_imaginary: float32 [64, 16, 64], P('tp'), may hold values from -0.5 to 0.5
- skip_weight: float32 [64, 16], P('tp'), may hold values from -3 to 3
- decay_shift: float32 [64, 4096], P('tp', 'sp'), may hold values from -2 to 0
- head_out_weight: bfloat16 [1024, 2048], P('tp'), may hold values from -0.375 to 0.375
- state_out_weight: bfloat16 [1024, 2048], P('tp'), may hold values from -0.375 to 0.375
Outputs:
- layer_out: bfloat16 [4096, 2048], P('sp', 'tp')
All inputs are finite; a program needn't handle non-finite values.
Results may differ from a plain program's by a relative error of at most 0.012.
Values may be sent and summed in bfloat16 or wider, within the bound.
A program may use at most 128 MiB of HBM per device.

v0:
```python
import jax
import jax.numpy as jnp
from jax import lax
from jax.sharding import PartitionSpec as P

HEAD_DIM = 64
Q_HEADS = 16
KV_HEADS = 8
GROUP_CH = 16
WINDOW = 128


NEG_FILL = -1e30


def shifted(value, axis, steps):
    count = lax.axis_size(axis)
    first, last = (max(0, -steps), min(count, count - steps))
    return lax.ppermute(value, axis, [(source, source + steps) for source in range(first, last)])


def carried_in(part, axis, combine, identity):
    place = lax.axis_index(axis)
    gathered = jax.tree.map(lambda a: lax.all_gather(a, axis), part)
    state = jax.tree.map(lambda a, e: jnp.zeros_like(a) + jnp.asarray(e, a.dtype), part, identity)

    def one(hop, state):
        return combine(
            state, jax.tree.map(lambda a: lax.dynamic_index_in_dim(a, hop, 0, False), gathered)
        )

    return lax.fori_loop(0, place, one, state)


def combine(earlier_pair, later_pair):
    prior_real, prior_imag, prior_sum_real, prior_sum_imag = earlier_pair
    after_real, after_imag, after_sum_real, after_sum_imag = later_pair
    return (
        prior_real * after_real - prior_imag * after_imag,
        prior_real * after_imag + prior_imag * after_real,
        after_real * prior_sum_real - after_imag * prior_sum_imag + after_sum_real,
        after_real * prior_sum_imag + after_imag * prior_sum_real + after_sum_imag,
    )


def within_segments(rows, segment, tile_width):
    extent = rows.shape[-1]
    leading = rows.shape[:-1]
    row_index = jnp.arange(tile_width, dtype=jnp.int32)[:, None]
    column_index = jnp.arange(tile_width, dtype=jnp.int32)[None, :]
    triangle = (
        (row_index // segment == column_index // segment) & (row_index <= column_index)
    ).astype(jnp.float32)
    flattened = rows.reshape(-1, tile_width)
    summed = jnp.dot(flattened, triangle, precision=lax.Precision.HIGHEST)
    return summed.reshape(leading + (extent,))


def attend(query_rows_all, key_value, sink_logit, head_gate):
    tok_rows = query_rows_all.shape[0]
    kv_width = key_value.shape[1] // 2
    kv_heads = kv_width // HEAD_DIM
    group_size = Q_HEADS // KV_HEADS
    blocks = tok_rows // WINDOW
    previous = shifted(key_value[tok_rows - WINDOW :], "sp", 1)
    joined = jnp.concatenate([previous, key_value], axis=0).reshape(
        blocks + 1, WINDOW, 2 * kv_width
    )
    banded = jnp.concatenate([joined[:-1], joined[1:]], axis=1)
    key_band = banded[..., :kv_width].reshape(blocks, 2 * WINDOW, kv_heads, HEAD_DIM)
    value_band = banded[..., kv_width:].reshape(blocks, 2 * WINDOW, kv_heads, HEAD_DIM)
    query_heads = query_rows_all.reshape(blocks, WINDOW, kv_heads, group_size, HEAD_DIM)
    scores = jnp.einsum(
        "nqkgd,nskd->nkgqs", query_heads, key_band, preferred_element_type=jnp.float32
    ) * HEAD_DIM ** (-0.5)
    query_index = jnp.arange(WINDOW, dtype=jnp.int32)[:, None]
    column = jnp.arange(2 * WINDOW, dtype=jnp.int32)[None, :]
    distance = WINDOW + query_index - column
    block_start = (
        lax.axis_index("sp") * tok_rows
        + jnp.arange(blocks, dtype=jnp.int32)[:, None, None] * WINDOW
    )
    allowed = (distance >= 0) & (distance < WINDOW) & (block_start - WINDOW + column >= 0)
    scores = jnp.where(allowed[:, None, None], scores, NEG_FILL)
    sink_col = sink_logit.reshape(kv_heads, group_size)[None, :, :, None, None]
    maxima = jnp.maximum(jnp.max(scores, axis=-1, keepdims=True), sink_col)
    exponent = jnp.exp(scores - maxima)
    totals = jnp.sum(exponent, axis=-1, keepdims=True) + jnp.exp(sink_col - maxima)
    weights = (exponent / totals).astype(jnp.bfloat16)
    attended = jnp.einsum(
        "nkgqs,nskd->nqkgd", weights, value_band, preferred_element_type=jnp.float32
    ).reshape(tok_rows, -1)
    return (jax.nn.sigmoid(head_gate.astype(jnp.float32)) * attended).astype(jnp.bfloat16)


def recur(
    state_input,
    state_gate,
    decay_real,
    decay_frequency,
    log_step,
    input_real,
    input_imaginary,
    output_real,
    output_imaginary,
    skip_weight,
    decay_shift,
):
    highest = lax.Precision.HIGHEST
    tok_rows = state_input.shape[0]
    groups = decay_real.shape[0]
    states = decay_real.shape[1]
    segment = min(16, tok_rows)
    tile_width = min(128, tok_rows)
    segment_count = tok_rows // segment
    stepsize = jnp.exp(log_step)[:, None]
    log_magnitude = decay_real * stepsize
    rotation = decay_frequency * stepsize
    magnitude = jnp.exp(log_magnitude)
    base_real = magnitude * jnp.cos(rotation)
    base_imag = magnitude * jnp.sin(rotation)
    denominator = decay_real * decay_real + decay_frequency * decay_frequency
    less_real = base_real - 1.0
    zoh_real = (less_real * decay_real + base_imag * decay_frequency) / denominator
    zoh_imag = (base_imag * decay_real - less_real * decay_frequency) / denominator
    drive_real = zoh_real[..., None] * input_real - zoh_imag[..., None] * input_imaginary
    drive_imag = zoh_real[..., None] * input_imaginary + zoh_imag[..., None] * input_real
    values = state_input.astype(jnp.float32).reshape(tok_rows, groups, GROUP_CH)
    push_real = jnp.einsum("tgp,gnp->gnt", values, drive_real, precision=highest)
    push_imag = jnp.einsum("tgp,gnp->gnt", values, drive_imag, precision=highest)
    counter = jnp.arange(1, segment + 1, dtype=jnp.float32)
    log_rate = counter * log_magnitude[..., None]
    angle_table = counter * rotation[..., None]
    repeats = (1, 1, segment_count)
    grow_rows = jnp.tile(jnp.exp(log_rate), repeats)
    shrink_rows = jnp.tile(jnp.exp(-log_rate), repeats)
    cosine = jnp.tile(jnp.cos(angle_table), repeats)
    sine_rows = jnp.tile(jnp.sin(angle_table), repeats)
    shift_sum = within_segments(decay_shift, segment, tile_width)
    inverse = jnp.exp(-shift_sum)[:, None, :] * shrink_rows
    weighted = jnp.stack(
        [
            inverse * (push_real * cosine + push_imag * sine_rows),
            inverse * (push_imag * cosine - push_real * sine_rows),
        ]
    )
    scaled = within_segments(weighted, segment, tile_width)
    grow = jnp.exp(shift_sum)[:, None, :] * grow_rows
    cum_real = grow * cosine
    cum_imag = grow * sine_rows
    local_real = cum_real * scaled[0] - cum_imag * scaled[1]
    local_imag = cum_real * scaled[1] + cum_imag * scaled[0]
    last = segment - 1
    segment_ends = (
        cum_real[..., last::segment],
        cum_imag[..., last::segment],
        local_real[..., last::segment],
        local_imag[..., last::segment],
    )
    inclusive = lax.associative_scan(combine, segment_ends, axis=2)
    summary = (
        inclusive[0][..., -1],
        inclusive[1][..., -1],
        inclusive[2][..., -1],
        inclusive[3][..., -1],
    )
    unity = jnp.ones_like(summary[0])
    nothing = jnp.zeros_like(summary[0])
    prefix = carried_in(summary, "sp", combine, (unity, nothing, nothing, nothing))
    carry_real, carry_imag = (prefix[2], prefix[3])
    ones_col = jnp.ones((groups, states, 1), jnp.float32)
    zero_col = jnp.zeros((groups, states, 1), jnp.float32)
    before_cum_real = jnp.concatenate([ones_col, inclusive[0][..., :-1]], axis=2)
    before_cum_imag = jnp.concatenate([zero_col, inclusive[1][..., :-1]], axis=2)
    before_real = jnp.concatenate([zero_col, inclusive[2][..., :-1]], axis=2)
    before_imag = jnp.concatenate([zero_col, inclusive[3][..., :-1]], axis=2)
    entry_real = (
        before_real
        + before_cum_real * carry_real[..., None]
        - before_cum_imag * carry_imag[..., None]
    )
    entry_imag = (
        before_imag
        + before_cum_real * carry_imag[..., None]
        + before_cum_imag * carry_real[..., None]
    )
    entry_real_rows = jnp.repeat(entry_real, segment, axis=2)
    entry_imag_rows = jnp.repeat(entry_imag, segment, axis=2)
    state_real = local_real + cum_real * entry_real_rows - cum_imag * entry_imag_rows
    state_imag = local_imag + cum_real * entry_imag_rows + cum_imag * entry_real_rows
    recurrent = (
        jnp.einsum("gpn,gnt->tgp", output_real, state_real, precision=highest)
        - jnp.einsum("gpn,gnt->tgp", output_imaginary, state_imag, precision=highest)
        + skip_weight[None] * values
    )
    recurrent = recurrent.reshape(tok_rows, groups * GROUP_CH)
    return (jax.nn.sigmoid(state_gate.astype(jnp.float32)) * jax.nn.gelu(recurrent)).astype(
        jnp.bfloat16
    )


def on_device(
    hidden,
    query_weight,
    key_weight,
    value_weight,
    head_gate_weight,
    state_in_weight,
    state_gate_weight,
    sink_logit,
    decay_real,
    decay_frequency,
    log_step,
    input_real,
    input_imaginary,
    output_real,
    output_imaginary,
    skip_weight,
    decay_shift,
    head_out_weight,
    state_out_weight,
):
    weight_list = (
        query_weight,
        key_weight,
        value_weight,
        head_gate_weight,
        state_in_weight,
        state_gate_weight,
    )
    portion = lax.all_gather(hidden, "tp", axis=1, tiled=True)
    sums = tuple(
        (jnp.dot(portion, weight, preferred_element_type=jnp.float32) for weight in weight_list)
    )
    query_rows_all, key_rows, value_rows, head_gate, state_input, state_gate = tuple(
        (running.astype(jnp.bfloat16) for running in sums)
    )
    key_value = jnp.concatenate([key_rows, value_rows], axis=1)
    head_mixed = attend(query_rows_all, key_value, sink_logit, head_gate)
    state_mixed = recur(
        state_input,
        state_gate,
        decay_real,
        decay_frequency,
        log_step,
        input_real,
        input_imaginary,
        output_real,
        output_imaginary,
        skip_weight,
        decay_shift,
    )
    head_columns, state_columns = (
        lax.all_to_all(head_out_weight, "tp", split_axis=1, concat_axis=0, tiled=True),
        lax.all_to_all(state_out_weight, "tp", split_axis=1, concat_axis=0, tiled=True),
    )
    layer_out = jnp.dot(
        lax.all_gather(head_mixed, "tp", axis=1, tiled=True),
        head_columns,
        preferred_element_type=jnp.float32,
    ) + jnp.dot(
        lax.all_gather(state_mixed, "tp", axis=1, tiled=True),
        state_columns,
        preferred_element_type=jnp.float32,
    )
    return layer_out.astype(jnp.bfloat16)


def solution(mesh):
    in_specs = (
        P("sp", "tp"),
        P(None, "tp"),
        P(None, "tp"),
        P(None, "tp"),
        P(None, "tp"),
        P(None, "tp"),
        P(None, "tp"),
        P("tp"),
        P("tp", None),
        P("tp", None),
        P("tp"),
        P("tp", None, None),
        P("tp", None, None),
        P("tp", None, None),
        P("tp", None, None),
        P("tp", None),
        P("tp", "sp"),
        P("tp", None),
        P("tp", None),
    )
    out_specs = P("sp", "tp")
    return jax.shard_map(
        on_device, mesh=mesh, in_specs=in_specs, out_specs=out_specs, check_vma=False
    )
```

profile of v0, /device:TPU:29, one launch (start us, length us, event | category | flops | bytes accessed | tf_op | source)
XLA Modules:
  0.0 353.2 jit_solution(15014803274585745117)
XLA Ops:
  7.3 3.9 %copy.108 = bf16[512,2048]{0,1:T(8,128)(2,1)} copy(bf16[512,2048]{1,0:T(8,128)(2,1)} %param.38) | data formatting | bytes 4194304 | tf_op args[17]
  11.2 5.6 %all-to-all-start = ((bf16[512,2,1024]{0,2,1:T(8,128)(2,1)}), bf16[512,2,1024]{0,2,1:T(8,128)(2,1)}, u32[]{:S(2)}, u32[]{:S(2)}) async-start(bf16[512,2,1024]{0,2,1:T(8,128)(2,1)} %bitcast.188), calls=%async_computation | async-start | bytes 4194304 | tf_op jit(solution)/shard_map/all_to_all | solution.py:254
  20.4 3.8 %copy.112 = f32[32,64,256]{2,1,0:T(8,128)} copy(f32[32,64,256]{1,2,0:T(8,128)} %bitcast.184) | data formatting | bytes 4194304 | tf_op jit(solution)/shard_map/tile | solution.py:137
  26.5 3.9 %copy.113 = f32[32,64,256]{2,1,0:T(8,128)} copy(f32[32,64,256]{1,2,0:T(8,128)} %bitcast.185) | data formatting | bytes 4194304 | tf_op jit(solution)/shard_map/tile | solution.py:138
  32.7 3.9 %copy.110 = f32[32,64,256]{2,1,0:T(8,128)} copy(f32[32,64,256]{1,2,0:T(8,128)} %bitcast.183) | data formatting | bytes 4194304 | tf_op jit(solution)/shard_map/tile | solution.py:136
  37.6 3.9 %copy.128 = bf16[512,2048]{0,1:T(8,128)(2,1)} copy(bf16[512,2048]{1,0:T(8,128)(2,1)} %param.39) | data formatting | bytes 4194304 | tf_op args[18]
  41.6 5.0 %all-to-all-start.1 = ((bf16[512,2,1024]{0,2,1:T(8,128)(2,1)}), bf16[512,2,1024]{0,2,1:T(8,128)(2,1)}, u32[]{:S(2)}, u32[]{:S(2)}) async-start(bf16[512,2,1024]{0,2,1:T(8,128)(2,1)} %bitcast.189), calls=%async_computation.1 | async-start | bytes 4194304 | tf_op jit(solution)/shard_map/all_to_all | solution.py:255
  46.6 4.0 %copy.109 = bf16[2,512,1024]{2,1,0:T(8,128)(2,1)} copy(bf16[2,512,1024]{1,2,0:T(8,128)(2,1)} %bitcast.13) | data formatting | bytes 4194304 | tf_op jit(solution)/shard_map/all_to_all | solution.py:254
  50.6 4.0 %copy.129 = bf16[2,512,1024]{2,1,0:T(8,128)(2,1)} copy(bf16[2,512,1024]{1,2,0:T(8,128)(2,1)} %bitcast.33) | data formatting | bytes 4194304 | tf_op jit(solution)/shard_map/all_to_all | solution.py:255
  55.4 2.7 convolution_convert_fusion
  61.4 3.9 %multiply_bitcast_fusion.1 = (f32[1,32,64,256]{3,2,1,0:T(8,128)S(1)}, f32[1,32,64,256]{3,2,1,0:T(8,128)S(1)}) fusion(f32[32,64,256]{2,1,0:T(8,128)S(1)} %fusion.35, f32[32,64,256]{2,1,0:T(8,128)} %copy.113, f32[32,64,256]{2,1,0:T(8,128)S(1)} %copy-done.2, f32[32,64,256]{2,1,0:T(8,128)} %copy.110, f32[32,256]{1,0:T(8,128)S(1)} %exp.74, ...), kind=kOutput, calls=%fused_computation.24 | convolution fusion | flops 105480192 | bytes 13156352 | tf_op jit(solution)/shard_map/tgp,gnp->gnt/dot_general | solution.py:129
  67.7 4.8 %reshape.251 = f32[8192,128]{1,0:T(8,128)} reshape(f32[2,32,64,256]{3,2,1,0:T(8,128)} %pad_maximum_fusion) | data formatting | bytes 8388608 | tf_op jit(solution)/shard_map/reshape | solution.py:54
  72.4 3.8 %fusion.52 = f32[8192,128]{1,0:T(8,128)S(1)} fusion(f32[8192,128]{1,0:T(8,128)} %reshape.251, s32[128]{0:T(128)S(1)} %and_select_fusion), kind=kOutput, calls=%fused_computation.129 | convolution fusion | flops 1610661888 | bytes 8389120 | tf_op jit(solution)/shard_map/dot_general | solution.py:55
  80.4 2.8 copy.116
  85.1 2.7 copy.117
  87.8 9.7 %multiply_add_fusion = (f32[32,64,256]{1,2,0:T(8,128)}, f32[32,64,256]{1,2,0:T(8,128)}, f32[32,64,256]{1,2,0:T(8,128)}, f32[32,64,256]{1,2,0:T(8,128)}) fusion(f32[32,64,256]{1,2,0:T(8,128)} %copy.116, f32[32,64,256]{1,2,0:T(8,128)} %copy.117, f32[32,64,16]{1,2,0:T(8,128)S(1)} %get-tuple-element.162, f32[32,64,16]{1,2,0:T(8,128)S(1)} %get-tuple-element.163, ...), kind=kLoop, calls=%fused_computation.20 | loop fusion | flops 4718592 | bytes 13008896 | tf_op jit(solution)/shard_map/add | solution.py:152
  97.5 2.9 slice.293
  100.6 2.9 slice.301
  103.7 2.9 slice.295
  106.7 2.9 slice.299
  127.6 28.8 %all-gather.3 = f32[512,64,1]{1,2,0:T(1,128)S(1)} all-gather(f32[32,64,1]{1,2,0:T(1,128)S(1)} %slice_add_fusion.10), channel_id=5, replica_groups=mesh['sp'=16,'tp'=2] {'sp'}, dimensions={0}, use_global_device_ids=true | all-gather | bytes 139264 | tf_op jit(solution)/shard_map/all_gather | solution.py:24
  157.0 32.2 %all-gather.1 = f32[512,64,1]{1,2,0:T(1,128)S(1)} all-gather(f32[32,64,1]{1,2,0:T(1,128)S(1)} %slice_add_fusion.11), channel_id=3, replica_groups=mesh['sp'=16,'tp'=2] {'sp'}, dimensions={0}, use_global_device_ids=true | all-gather | bytes 139264 | tf_op jit(solution)/shard_map/all_gather | solution.py:24
  189.4 30.3 %all-gather = f32[512,64,1]{1,2,0:T(1,128)S(1)} all-gather(f32[32,64,1]{1,2,0:T(1,128)S(1)} %slice.616), channel_id=2, replica_groups=mesh['sp'=16,'tp'=2] {'sp'}, dimensions={0}, use_global_device_ids=true | all-gather | bytes 139264 | tf_op jit(solution)/shard_map/all_gather | solution.py:24
  219.7 10.3 %pad.290 = f32[32,64,15]{1,2,0:T(8,128)} pad(f32[32,64,8]{1,2,0:T(8,128)S(1)} %add.395, f32[]{:T(128)} %constant.81.clone.1), padding=0_0_0x0_0_0x0_0_1 | pad | bytes 188420
  230.9 34.0 %all-gather.2 = f32[512,64,1]{1,2,0:T(1,128)} all-gather(f32[32,64,1]{1,2,0:T(1,128)S(1)} %slice.618), channel_id=4, replica_groups=mesh['sp'=16,'tp'=2] {'sp'}, dimensions={0}, use_global_device_ids=true | all-gather | bytes 139264 | tf_op jit(solution)/shard_map/all_gather | solution.py:24
  264.9 10.6 %while.15 = (s32[]{:T(128)}, f32[32,64]{1,0:T(8,128)S(1)}, f32[32,64]{1,0:T(8,128)S(1)}, s32[]{:T(128)}, f32[16,32,64]{2,1,0:T(8,128)S(1)}, /*index=5*/f32[16,32...) while((s32[]{:T(128)}, f32[32,64]{1,0:T(8,128)S(1)}, ...), condition=%wide.region_3.4_spmd, body=%wide.region_2.3_spmd.sunk | while | flops 16389 | bytes 65683 | solution.py:32
  277.3 5.0 %fusion.4 = (f32[32,64,256]{1,2,0:T(8,128)S(1)}, f32[32,64,256]{1,2,0:T(8,128)S(1)}) fusion(f32[32,64,256]{1,2,0:T(8,128)} %get-tuple-element.97, f32[32,64,16]{1,2,0:T(8,128)S(1)} %get-tuple-element.108, f32[32,64,16]{1,2,0:T(8,128)S(1)} %get-tuple-element.107, f32[32,64,16]{1,2,0:T(8,128)S(1)} %get-tuple-element.162, ...), kind=kLoop, calls=%fused_computation.14 | loop fusion | flops 5767168 | bytes 9076736 | tf_op jit(solution)/shard_map/add | solution.py:190
  282.3 3.8 %fusion.73 = f32[32,256,16]{1,2,0:T(8,128)S(1)} fusion(f32[32,64,256]{1,2,0:T(8,128)S(1)} %get-tuple-element.102, f32[32,16,64]{2,1,0:T(8,128)S(1)} %copy-done.14), kind=kOutput, calls=%fused_computation.196 | convolution fusion | flops 100663296 | bytes 2752512 | tf_op jit(solution)/shard_map/gpn,gnt->tgp/dot_general | solution.py:192
  286.1 3.8 %fusion.11 = f32[256,32,16]{0,2,1:T(8,128)S(1)} fusion(f32[32,256,16]{1,2,0:T(8,128)S(1)} %fusion.73, f32[32,64,256]{1,2,0:T(8,128)S(1)} %get-tuple-element.101, f32[32,16,64]{2,1,0:T(8,128)S(1)} %copy-done.15, bf16[256,32,16]{0,2,1:T(8,128)(2,1)S(1)} %bitcast.192, f32[32,16]{1,0:T(8,128)S(1)} %copy.122), kind=kOutput, calls=%fused_computation.33 | convolution fusion | flops 101187584 | bytes 3540992 | tf_op jit(solution)/shard_map/gpn,gnt->tgp/dot_general | solution.py:193
  293.3 4.6 %collective-permute-start = (bf16[128,512]{0,1:T(8,128)(2,1)S(1)}, bf16[128,512]{0,1:T(8,128)(2,1)S(1)}, u32[]{:S(2)}, u32[]{:S(2)}) collective-permute-start(bf16[128,512]{0,1:T(8,128)(2,1)S(1)} %fusion.43), channel_id=1, source_target_pairs={{0,2},{2,4},{4,6},{6,8},{8,10},{10,12},{12,14},{14,16},{16,18},{18... | collective-permute-start | bytes 393224 | tf_op jit(solution)/shard_map/ppermute | solution.py:19
  301.4 30.6 %all_gather.27 = bf16[256,1024]{1,0:T(8,128)(2,1)} all-gather(bf16[256,512]{1,0:T(8,128)(2,1)S(1)} %fusion.25), channel_id=1, replica_groups=mesh['sp'=16,'tp'=2] {'tp'}, dimensions={1}, use_global_device_ids=true | all-gather | bytes 786432 | tf_op jit(solution)/shard_map/all_gather | solution.py:262
  339.1 2.6 fusion.18
  (243 shorter events, 72.3 us)
Async XLA Ops:
  6.5 48.9 %copy-start = (bf16[2048,512]{1,0:T(8,128)(2,1)S(1)}, bf16[2048,512]{1,0:T(8,128)(2,1)}, u32[]{:S(2)}) copy-start(bf16[2048,512]{1,0:T(8,128)(2,1)} %param.26) | copy-start | bytes 6291460
  6.5 48.9 %all-gather.6.cloned.1.call-start = ((), (), s32[]{:S(2)}) async-start(), calls=%async_computation.2 | async-start | bytes 1572864 | tf_op jit(solution)/shard_map/all_gather | solution.py:231
  11.2 5.6 %copy-start.30 = (f32[32]{0:T(128)S(1)}, f32[32]{0:T(128)}, u32[]{:S(2)}) copy-start(f32[32]{0:T(128)} %param.31) | copy-start | bytes 388
  11.2 5.6 %copy-start.25 = (f32[32,64]{1,0:T(8,128)S(1)}, f32[32,64]{1,0:T(8,128)}, u32[]{:S(2)}) copy-start(f32[32,64]{1,0:T(8,128)} %param.30) | copy-start | bytes 24580
  11.2 5.6 %copy-start.26 = (f32[32,64]{1,0:T(8,128)S(1)}, f32[32,64]{1,0:T(8,128)}, u32[]{:S(2)}) copy-start(f32[32,64]{1,0:T(8,128)} %param.29) | copy-start | bytes 24580
  11.2 30.4 %all-to-all-start = ((bf16[512,2,1024]{0,2,1:T(8,128)(2,1)}), bf16[512,2,1024]{0,2,1:T(8,128)(2,1)}, u32[]{:S(2)}, u32[]{:S(2)}) async-start(bf16[512,2,1024]{0,2,1:T(8,128)(2,1)} %bitcast.188), calls=%async_computation | async-start | bytes 4194304 | tf_op jit(solution)/shard_map/all_to_all | solution.py:254
  32.7 3.9 %copy-start.23 = (f32[32,256]{1,0:T(8,128)S(1)}, f32[32,256]{1,0:T(8,128)}, u32[]{:S(2)}) copy-start(f32[32,256]{1,0:T(8,128)} %param.37) | copy-start | bytes 98308
  32.7 4.2 %copy-start.27 = (f32[32,16]{0,1:T(8,128)S(1)}, f32[32,16]{0,1:T(8,128)}, u32[]{:S(2)}) copy-start(f32[32,16]{0,1:T(8,128)} %param.36) | copy-start | bytes 6148
  32.7 4.3 %copy-start.28 = (f32[8]{0:T(128)S(1)}, f32[8]{0:T(128)}, u32[]{:S(2)}) copy-start(f32[8]{0:T(128)} %param.28) | copy-start | bytes 100
  36.9 50.9 %copy-start.12 = (f32[32,256]{1,0:T(8,128)}, f32[32,256]{1,0:T(8,128)S(1)}, u32[]{:S(2)}) copy-start(f32[32,256]{1,0:T(8,128)S(1)} %exp.69) | copy-start | bytes 98308
  41.6 9.0 %all-to-all-start.1 = ((bf16[512,2,1024]{0,2,1:T(8,128)(2,1)}), bf16[512,2,1024]{0,2,1:T(8,128)(2,1)}, u32[]{:S(2)}, u32[]{:S(2)}) async-start(bf16[512,2,1024]{0,2,1:T(8,128)(2,1)} %bitcast.189), calls=%async_computation.1 | async-start | bytes 4194304 | tf_op jit(solution)/shard_map/all_to_all | solution.py:255
  55.4 3.9 %copy-start.8 = (f32[32,64,16]{1,2,0:T(8,128)S(1)}, f32[32,64,16]{1,2,0:T(8,128)}, u32[]{:S(2)}) copy-start(f32[32,64,16]{1,2,0:T(8,128)} %param.32) | copy-start | bytes 393220
  58.1 3.3 copy-start.2
  59.3 2.1 copy-start.9
  114.4 7.7 %copy-start.22 = (f32[32,64,1]{1,2,0:T(1,128)S(1)}, f32[32,64,1]{1,2,0:T(1,128)}, u32[]{:S(2)}) copy-start(f32[32,64,1]{1,2,0:T(1,128)} %get-tuple-element.142) | copy-start | bytes 24580
  122.9 2.8 copy-start.21
  125.4 1.3 copy-start.19
  126.6 30.0 %copy-start.20 = (f32[32,64,1]{1,2,0:T(1,128)S(1)}, f32[32,64,1]{1,2,0:T(1,128)}, u32[]{:S(2)}) copy-start(f32[32,64,1]{1,2,0:T(1,128)} %slice.429) | copy-start | bytes 24580
  189.2 87.2 %copy-start.18 = (f32[32,64,1]{1,2,0:T(1,128)S(1)}, f32[32,64,1]{1,2,0:T(1,128)}, u32[]{:S(2)}) copy-start(f32[32,64,1]{1,2,0:T(1,128)} %slice.408) | copy-start | bytes 24580
  264.9 11.8 %copy-start.17 = (f32[32,64,1]{1,2,0:T(1,128)S(1)}, f32[32,64,1]{1,2,0:T(1,128)}, u32[]{:S(2)}) copy-start(f32[32,64,1]{1,2,0:T(1,128)} %slice.379) | copy-start | bytes 24580
  277.3 5.0 %copy-start.14 = (f32[32,16,64]{2,1,0:T(8,128)S(1)}, f32[32,16,64]{2,1,0:T(8,128)}, u32[]{:S(2)}) copy-start(f32[32,16,64]{2,1,0:T(8,128)} %param.34) | copy-start | bytes 393220
  282.3 3.8 %copy-start.15 = (f32[32,16,64]{2,1,0:T(8,128)S(1)}, f32[32,16,64]{2,1,0:T(8,128)}, u32[]{:S(2)}) copy-start(f32[32,16,64]{2,1,0:T(8,128)} %param.35) | copy-start | bytes 393220
  286.0 4.8 %copy-start.5 = (bf16[256,2048]{1,0:T(8,128)(2,1)S(1)}, bf16[256,2048]{1,0:T(8,128)(2,1)}, u32[]{:S(2)}) copy-start(bf16[256,2048]{1,0:T(8,128)(2,1)} %all-gather.6.cloned.1.call-done) | copy-start | bytes 3145732
  289.8 2.9 copy-start.10
  290.8 7.1 %copy-start.29 = (bf16[2048,512]{1,0:T(8,128)(2,1)S(1)}, bf16[2048,512]{1,0:T(8,128)(2,1)}, u32[]{:S(2)}) copy-start(bf16[2048,512]{1,0:T(8,128)(2,1)} %param.22) | copy-start | bytes 6291460
  293.3 5.7 %copy-start.11 = (f32[256,512]{1,0:T(8,128)S(1)}, f32[256,512]{1,0:T(8,128)}, u32[]{:S(2)}) copy-start(f32[256,512]{1,0:T(8,128)} %copy.127) | copy-start | bytes 1572868
  293.3 38.8 %collective-permute-start = (bf16[128,512]{0,1:T(8,128)(2,1)S(1)}, bf16[128,512]{0,1:T(8,128)(2,1)S(1)}, u32[]{:S(2)}, u32[]{:S(2)}) collective-permute-start(bf16[128,512]{0,1:T(8,128)(2,1)S(1)} %fusion.43), channel_id=1, source_target_pairs={{0,2},{2,4},{4,6},{6,8},{8,10},{10,12},{12,14},{14,16},{16,18},{18... | collective-permute-start | bytes 393224 | tf_op jit(solution)/shard_map/ppermute | solution.py:19
  335.6 3.5 copy-start.6
  339.1 5.0 %copy-start.3 = (bf16[2,512,1024]{2,1,0:T(8,128)(2,1)S(1)}, bf16[2,512,1024]{2,1,0:T(8,128)(2,1)}, u32[]{:S(2)}) copy-start(bf16[2,512,1024]{2,1,0:T(8,128)(2,1)} %copy.109) | copy-start | bytes 6291460
  341.7 3.1 copy-start.4
  341.7 3.1 copy-start.7
  344.8 1.6 copy-start.1
  (3 other events, 3.0 us)
Sparse Core Ops, SparseCore 0:
  8.9 11.2 all-gather.5
where the time goes:
time: 355 us; the launch traced here: 353 us
  blocking collectives  158 us (45%)
  local copies, waits for them, and re-layouts  96.8 us (27%)
  other arithmetic  34.7 us (10%)
  matrix products  32.5 us (9%)
  starting transfers between devices  15.2 us (4%)
  between operations  14.6 us (4%)
    all_gather x4, blocking collectives, carried_in(): gathered = jax.tree.map(lambda a: lax.all_gather(a, axis), part)  125 us
    all_gather x1, blocking collectives, on_device(): lax.all_gather(state_mixed, 'tp', axis=1, tiled=True)  30.6 us
    unnamed x70, local copies, waits for them, and re-layouts  19.3 us
    add x17, other arithmetic, combine(): after_real * prior_sum_imag + after_imag * prior_sum_real + after_sum_imag  11.2 us
    dot_general x6, matrix products, on_device(): jnp.dot(portion, weight, preferred_element_type=jnp.float32)  10.9 us
    add x1, other arithmetic, recur(): local_imag = cum_real * scaled[1] + cum_imag * scaled[0]  9.67 us
    squeeze x4, local copies, waits for them, and re-layouts, recur(): local_real = cum_real * scaled[0] - cum_imag * scaled[1]  9.31 us
    pad x22, local copies, waits for them, and re-layouts, recur(): inclusive = lax.associative_scan(combine, segment_ends, axis=2)  7.17 us
  transfers between devices with their start and end apart: 4, of which 0 were waited for; matrix products, arithmetic and copies ran while one was open for 12% of the time, Pallas kernels for 0%

commit v1 on v0

v1 whole, which is shorter than its diff:
```python
import functools

import jax
import jax.numpy as jnp
import numpy as np
from jax import lax
from jax.experimental import pallas as pl
from jax.experimental.pallas import tpu as pltpu
from jax.sharding import PartitionSpec as P

HEAD_DIM = 64
Q_HEADS = 16
KV_HEADS = 8
GROUP_CH = 16
WINDOW = 128
CHUNK = 16
LANES = 128

NEG_FILL = -1e30
MESH = pl.DeviceIdType.MESH
VMEM = pl.BlockSpec(memory_space=pltpu.VMEM)
BF16 = jnp.bfloat16
F32 = jnp.float32


def shifted(value, axis, steps):
    count = lax.axis_size(axis)
    first, last = (max(0, -steps), min(count, count - steps))
    return lax.ppermute(value, axis, [(source, source + steps) for source in range(first, last)])


def params(collective_id=None):
    extra = {} if collective_id is None else {"collective_id": collective_id, "has_side_effects": True}
    return pltpu.CompilerParams(vmem_limit_bytes=60 * 1024 * 1024, **extra)


def hidden_kernel(own_ref, full_ref, send_sem, recv_sem):
    me = lax.axis_index("tp")
    other = 1 - me
    width = own_ref.shape[1]
    barrier = pltpu.get_barrier_semaphore()
    pl.semaphore_signal(barrier, inc=1, device_id={"tp": other}, device_id_type=MESH)
    pl.semaphore_wait(barrier, 1)
    mine = pl.ds(pl.multiple_of(me * width, LANES), width)
    copy = pltpu.make_async_remote_copy(
        src_ref=own_ref,
        dst_ref=full_ref.at[:, mine],
        send_sem=send_sem,
        recv_sem=recv_sem,
        device_id={"tp": other},
        device_id_type=MESH,
    )
    copy.start()
    full_ref[:, mine] = own_ref[...]
    copy.wait()


def gather_hidden(hidden):
    rows, width = hidden.shape
    return pl.pallas_call(
        hidden_kernel,
        out_shape=jax.ShapeDtypeStruct((rows, 2 * width), hidden.dtype),
        in_specs=[VMEM],
        out_specs=VMEM,
        scratch_shapes=[pltpu.SemaphoreType.DMA, pltpu.SemaphoreType.DMA],
        compiler_params=params(0),
        name="hidden_exchange",
    )(hidden)


def output_kernel(head_ref, state_ref, how_ref, sow_ref, out_ref, away, landed, send_sem, recv_sem):
    me = lax.axis_index("tp")
    other = 1 - me
    rows, width = out_ref.shape
    pieces = away.shape[0]
    step = width // pieces
    barrier = pltpu.get_barrier_semaphore()
    pl.semaphore_signal(barrier, inc=1, device_id={"tp": other}, device_id_type=MESH)
    pl.semaphore_wait(barrier, 1)

    def product(owner, piece):
        columns = pl.ds(pl.multiple_of(owner * width + piece * step, LANES), step)
        return jnp.dot(head_ref[...], how_ref[:, columns], preferred_element_type=F32) + jnp.dot(
            state_ref[...], sow_ref[:, columns], preferred_element_type=F32
        )

    copies = [
        pltpu.make_async_remote_copy(
            src_ref=away.at[piece],
            dst_ref=landed.at[piece],
            send_sem=send_sem.at[piece],
            recv_sem=recv_sem.at[piece],
            device_id={"tp": other},
            device_id_type=MESH,
        )
        for piece in range(pieces)
    ]
    for piece in range(pieces):
        away[piece] = product(other, piece).astype(away.dtype)
        if piece > 0:
            copies[piece - 1].start()
    own = [product(me, 0)]
    copies[pieces - 1].start()
    for piece in range(pieces):
        total = own[0] if piece == 0 else product(me, piece)
        copies[piece].wait()
        out_ref[:, pl.ds(piece * step, step)] = (total + landed[piece].astype(F32)).astype(out_ref.dtype)


def project_out(head_mixed, state_mixed, head_out_weight, state_out_weight):
    rows = head_mixed.shape[0]
    width = head_out_weight.shape[1] // 2
    pieces = 4
    return pl.pallas_call(
        output_kernel,
        out_shape=jax.ShapeDtypeStruct((rows, width), BF16),
        in_specs=[VMEM] * 4,
        out_specs=VMEM,
        scratch_shapes=[
            pltpu.VMEM((pieces, rows, width // pieces), F32),
            pltpu.VMEM((pieces, rows, width // pieces), F32),
            pltpu.SemaphoreType.DMA((pieces,)),
            pltpu.SemaphoreType.DMA((pieces,)),
        ],
        compiler_params=params(1),
        name="output_projection",
    )(head_mixed, state_mixed, head_out_weight, state_out_weight)


def turn(value, same, swapped):
    return value * same + pltpu.roll(value, value.shape[1] // 2, 1) * swapped


def local_kernel(
    uw_ref, gtab_ref, dtab_ref, e_ref, et_ref, a16_ref, b16_ref, tail_ref, whole_ref, tile_ref,
    intra_ref, g_ref, pushed_ref, msg_ref,
):
    groups = gtab_ref.shape[0]
    chunks = uw_ref.shape[0] // groups
    span = uw_ref.shape[1]
    row = lax.broadcasted_iota(jnp.int32, (span, span), 0) // GROUP_CH
    column = lax.broadcasted_iota(jnp.int32, (span, span), 1) // GROUP_CH
    causal = row <= column
    batch = 4

    def one(step, carry):
        ids = [step * batch + k for k in range(batch)]
        wide = [jnp.dot(gtab_ref[g], e_ref[...], preferred_element_type=F32) for g in ids]
        tall = [jnp.dot(et_ref[...], dtab_ref[g], preferred_element_type=F32) for g in ids]
        out_side = [
            (x[:, :span] * x[:, span : 2 * span] + x[:, 2 * span : 3 * span] * x[:, 3 * span :]).astype(BF16)
            for x in wide
        ]
        in_side = [
            (x[:span] * x[span : 2 * span] + x[2 * span : 3 * span] * x[3 * span :]).astype(BF16)
            for x in tall
        ]
        for g, value in zip(ids, out_side):
            g_ref[g] = value
        table = [
            jnp.where(causal, jnp.dot(a, b, preferred_element_type=F32), 0.0).astype(BF16)
            for a, b in zip(in_side, out_side)
        ]
        for g, t, d in zip(ids, table, in_side):
            rows = pl.ds(pl.multiple_of(g * chunks, chunks), chunks)
            u = uw_ref[rows, :]
            intra_ref[rows, :] = jnp.dot(u, t, preferred_element_type=F32)
            pushed_ref[rows, :] = jnp.dot(u, d, preferred_element_type=F32)
        return carry

    lax.fori_loop(0, groups // batch, one, 0)
    same, swapped = a16_ref[...], b16_ref[...]
    state = jnp.zeros((groups, pushed_ref.shape[1]), F32)
    for c in range(chunks):
        rows = pl.ds(c, groups, stride=chunks)
        local = tail_ref[rows, :] * turn(pushed_ref[rows, :], same, swapped)
        pushed_ref[rows, :] = local
        state = whole_ref[rows, :] * turn(state, same, swapped) + local
    msg_ref[:groups, :] = state
    msg_ref[groups:, :] = tile_ref[...]


def carry_kernel(msg_ref, same_ref, swapped_ref, carry_ref, landed, send_sem, recv_sem):
    me = lax.axis_index("sp")
    count = lax.axis_size("sp")
    groups = carry_ref.shape[0]
    barrier = pltpu.get_barrier_semaphore()

    def greet(hop, x):
        pl.semaphore_signal(
            barrier, inc=1, device_id={"sp": lax.rem(me + hop, count)}, device_id_type=MESH
        )
        return x

    lax.fori_loop(1, count, greet, 0)
    pl.semaphore_wait(barrier, count - 1)

    def outgoing(target):
        return pltpu.make_async_remote_copy(
            src_ref=msg_ref,
            dst_ref=landed.at[me],
            send_sem=send_sem.at[target],
            recv_sem=recv_sem.at[me],
            device_id={"sp": target},
            device_id_type=MESH,
        )

    def incoming(source):
        return pltpu.make_async_remote_copy(
            src_ref=msg_ref,
            dst_ref=landed.at[source],
            send_sem=send_sem.at[source],
            recv_sem=recv_sem.at[source],
            device_id={"sp": source},
            device_id_type=MESH,
        )

    def send(target, x):
        outgoing(target).start()
        return x

    lax.fori_loop(me + 1, count, send, 0)
    same, swapped = same_ref[...], swapped_ref[...]
    pick = lax.broadcasted_iota(jnp.int32, (groups, LANES), 0) == lax.broadcasted_iota(
        jnp.int32, (groups, LANES), 1
    )

    def absorb(source, state):
        incoming(source).wait_recv()
        shift_row = landed[source, pl.ds(groups, 1), :]
        total = jnp.sum(jnp.where(pick, shift_row, 0.0), axis=1, keepdims=True)
        return jnp.exp(total) * turn(state, same, swapped) + landed[source, pl.ds(0, groups), :]

    carry_ref[...] = lax.fori_loop(0, me, absorb, jnp.zeros(carry_ref.shape, F32))

    def drain(target, x):
        outgoing(target).wait_send()
        return x

    lax.fori_loop(me + 1, count, drain, 0)


def finish_kernel(
    carry_ref, pushed_ref, intra_ref, g_ref, wout_ref, a16_ref, b16_ref, head_ref, whole_ref,
    out_ref, entry,
):
    groups = g_ref.shape[0]
    chunks = pushed_ref.shape[0] // groups
    same, swapped = a16_ref[...], b16_ref[...]
    state = carry_ref[...]
    for c in range(chunks):
        rows = pl.ds(c, groups, stride=chunks)
        entry[rows, :] = head_ref[rows, :] * state
        state = whole_ref[rows, :] * turn(state, same, swapped) + pushed_ref[rows, :]
    batch = 8

    def one(step, x):
        for k in range(batch):
            g = step * batch + k
            rows = pl.ds(pl.multiple_of(g * chunks, chunks), chunks)
            far = jnp.dot(entry[rows, :].astype(BF16), g_ref[g], preferred_element_type=F32)
            out_ref[rows, :] = (wout_ref[rows, :] * (intra_ref[rows, :] + far)).astype(out_ref.dtype)
        return x

    lax.fori_loop(0, groups // batch, one, 0)


def spread_matrix():
    span = CHUNK * GROUP_CH
    column = np.arange(span)
    by_step = (np.arange(CHUNK)[:, None] == column[None] // GROUP_CH).astype(np.float32)
    by_channel = (np.arange(GROUP_CH)[:, None] == column[None] % GROUP_CH).astype(np.float32)
    out = np.zeros((8 * CHUNK, 4 * span), np.float32)
    for kind in range(4):
        block = by_channel if kind % 2 else by_step
        for half in range(2):
            first = (2 * kind + half) * CHUNK
            out[first : first + CHUNK, kind * span : (kind + 1) * span] = block
    return out


def shift_matrix(states2):
    span = CHUNK * GROUP_CH
    step = np.arange(CHUNK)
    upto = (step[:, None] <= (np.arange(span) // GROUP_CH)[None]).astype(np.float32)
    ref = (step < CHUNK // 2).astype(np.float32)[:, None]
    relative = upto - ref
    return np.concatenate(
        [relative, np.repeat(ref, states2, 1), np.ones((CHUNK, states2), np.float32)], axis=1
    )


def halves(value):
    high = lax.reduce_precision(value, 8, 7)
    return [high.astype(BF16), (value - high).astype(BF16)]


def tables(decay_real, decay_frequency, log_step, input_real, input_imaginary, output_real, output_imaginary, chunks):
    stepsize = jnp.exp(log_step)[:, None]
    log_magnitude = decay_real * stepsize
    rotation = decay_frequency * stepsize
    magnitude = jnp.exp(log_magnitude)
    base_real = magnitude * jnp.cos(rotation)
    base_imag = magnitude * jnp.sin(rotation)
    denominator = decay_real * decay_real + decay_frequency * decay_frequency
    less_real = base_real - 1.0
    zoh_real = (less_real * decay_real + base_imag * decay_frequency) / denominator
    zoh_imag = (base_imag * decay_real - less_real * decay_frequency) / denominator
    counter = jnp.arange(1, CHUNK + 1, dtype=F32)[:, None, None]
    angle = counter * rotation
    cosine, sine = jnp.cos(angle), jnp.sin(angle)
    grow = jnp.exp(counter * log_magnitude)
    shrink = jnp.exp(-counter * log_magnitude)
    power_real, power_imag = grow * cosine, grow * sine
    inverse_real, inverse_imag = shrink * cosine, -shrink * sine
    real_t = power_real.transpose(1, 2, 0)
    imag_t = power_imag.transpose(1, 2, 0)
    out_real = output_real.transpose(0, 2, 1)
    out_imag = output_imaginary.transpose(0, 2, 1)
    stack = lambda a, b: jnp.concatenate([a, b], axis=1)
    x1 = stack(real_t, -imag_t)
    x2 = stack(out_real, out_real)
    x3 = stack(-imag_t, -real_t)
    x4 = stack(out_imag, out_imag)
    gtab = jnp.concatenate([h for x in (x1, x2, x3, x4) for h in halves(x)], axis=2)
    drive_real = zoh_real[..., None] * input_real - zoh_imag[..., None] * input_imaginary
    drive_imag = zoh_real[..., None] * input_imaginary + zoh_imag[..., None] * input_real
    drive_real = drive_real.transpose(0, 2, 1)
    drive_imag = drive_imag.transpose(0, 2, 1)
    inv_real = inverse_real.transpose(1, 0, 2)
    inv_imag = inverse_imag.transpose(1, 0, 2)
    beside = lambda a, b: jnp.concatenate([a, b], axis=2)
    z1 = beside(inv_real, inv_real)
    z2 = beside(drive_real, drive_imag)
    z3 = beside(-inv_imag, inv_imag)
    z4 = beside(drive_imag, drive_real)
    dtab = jnp.concatenate([h for z in (z1, z2, z3, z4) for h in halves(z)], axis=1)
    last_real, last_imag = power_real[-1], power_imag[-1]
    all_real, all_imag = last_real, last_imag
    for _ in range(chunks - 1):
        all_real, all_imag = (
            all_real * last_real - all_imag * last_imag,
            all_real * last_imag + all_imag * last_real,
        )
    pair = lambda r, i: (jnp.concatenate([r, r], axis=1), jnp.concatenate([-i, i], axis=1))
    return gtab, dtab, pair(last_real, last_imag), pair(all_real, all_imag)


def recur(
    state_input, state_gate, decay_real, decay_frequency, log_step, input_real, input_imaginary,
    output_real, output_imaginary, skip_weight, decay_shift,
):
    tok_rows = state_input.shape[0]
    groups, states = decay_real.shape
    chunks = tok_rows // CHUNK
    span = CHUNK * GROUP_CH
    states2 = 2 * states
    gtab, dtab, (a16, b16), (a_all, b_all) = tables(
        decay_real, decay_frequency, log_step, input_real, input_imaginary, output_real,
        output_imaginary, chunks,
    )
    sums = jnp.dot(
        decay_shift.reshape(groups * chunks, CHUNK), jnp.asarray(shift_matrix(states2)),
        precision=lax.Precision.HIGHEST,
    )
    relative = sums[:, :span]
    head = jnp.exp(sums[:, span : span + states2])
    whole_log = sums[:, span + states2 :]
    whole = jnp.exp(whole_log)
    tail = jnp.exp(whole_log - sums[:, span : span + states2])
    weight_out = jnp.exp(relative)
    tile = jnp.zeros((8, LANES), F32).at[0, :groups].set(jnp.sum(decay_shift, axis=1))
    u = (
        state_input.reshape(chunks, CHUNK, groups, GROUP_CH)
        .transpose(2, 0, 1, 3)
        .reshape(groups * chunks, span)
    )
    uw = (u.astype(F32) * jnp.exp(-relative)).astype(BF16)
    spread = spread_matrix()
    rows = groups * chunks
    intra, g_out, pushed, message = pl.pallas_call(
        local_kernel,
        out_shape=(
            jax.ShapeDtypeStruct((rows, span), F32),
            jax.ShapeDtypeStruct((groups, states2, span), BF16),
            jax.ShapeDtypeStruct((rows, states2), F32),
            jax.ShapeDtypeStruct((groups + 8, LANES), F32),
        ),
        in_specs=[VMEM] * 10,
        out_specs=(VMEM,) * 4,
        compiler_params=params(),
        name="state_local",
    )(uw, gtab, dtab, jnp.asarray(spread, BF16), jnp.asarray(spread.T, BF16), a16, b16, tail, whole, tile)
    count = lax.axis_size("sp")
    carry = pl.pallas_call(
        carry_kernel,
        out_shape=jax.ShapeDtypeStruct((groups, states2), F32),
        in_specs=[VMEM] * 3,
        out_specs=VMEM,
        scratch_shapes=[
            pltpu.VMEM((count, groups + 8, LANES), F32),
            pltpu.SemaphoreType.DMA((count,)),
            pltpu.SemaphoreType.DMA((count,)),
        ],
        compiler_params=params(2),
        name="state_carry",
    )(message, a_all, b_all)
    recurrent = pl.pallas_call(
        finish_kernel,
        out_shape=jax.ShapeDtypeStruct((rows, span), F32),
        in_specs=[VMEM] * 9,
        out_specs=VMEM,
        scratch_shapes=[pltpu.VMEM((rows, states2), F32)],
        compiler_params=params(),
        name="state_finish",
    )(carry, pushed, intra, g_out, weight_out, a16, b16, head, whole)
    recurrent = (
        recurrent.reshape(groups, chunks, CHUNK, GROUP_CH)
        .transpose(1, 2, 0, 3)
        .reshape(tok_rows, groups * GROUP_CH)
    )
    recurrent = recurrent + skip_weight.reshape(1, -1) * state_input.astype(F32)
    return (jax.nn.sigmoid(state_gate.astype(F32)) * jax.nn.gelu(recurrent)).astype(BF16)


def attend(query_rows_all, key_value, sink_logit, head_gate):
    tok_rows = query_rows_all.shape[0]
    kv_width = key_value.shape[1] // 2
    kv_heads = kv_width // HEAD_DIM
    group_size = Q_HEADS // KV_HEADS
    blocks = tok_rows // WINDOW
    previous = shifted(key_value[tok_rows - WINDOW :], "sp", 1)
    joined = jnp.concatenate([previous, key_value], axis=0).reshape(
        blocks + 1, WINDOW, 2 * kv_width
    )
    banded = jnp.concatenate([joined[:-1], joined[1:]], axis=1)
    key_band = banded[..., :kv_width].reshape(blocks, 2 * WINDOW, kv_heads, HEAD_DIM)
    value_band = banded[..., kv_width:].reshape(blocks, 2 * WINDOW, kv_heads, HEAD_DIM)
    query_heads = query_rows_all.reshape(blocks, WINDOW, kv_heads, group_size, HEAD_DIM)
    scores = jnp.einsum(
        "nqkgd,nskd->nkgqs", query_heads, key_band, preferred_element_type=jnp.float32
    ) * HEAD_DIM ** (-0.5)
    query_index = jnp.arange(WINDOW, dtype=jnp.int32)[:, None]
    column = jnp.arange(2 * WINDOW, dtype=jnp.int32)[None, :]
    distance = WINDOW + query_index - column
    block_start = (
        lax.axis_index("sp") * tok_rows
        + jnp.arange(blocks, dtype=jnp.int32)[:, None, None] * WINDOW
    )
    allowed = (distance >= 0) & (distance < WINDOW) & (block_start - WINDOW + column >= 0)
    scores = jnp.where(allowed[:, None, None], scores, NEG_FILL)
    sink_col = sink_logit.reshape(kv_heads, group_size)[None, :, :, None, None]
    maxima = jnp.maximum(jnp.max(scores, axis=-1, keepdims=True), sink_col)
    exponent = jnp.exp(scores - maxima)
    totals = jnp.sum(exponent, axis=-1, keepdims=True) + jnp.exp(sink_col - maxima)
    weights = (exponent / totals).astype(jnp.bfloat16)
    attended = jnp.einsum(
        "nkgqs,nskd->nqkgd", weights, value_band, preferred_element_type=jnp.float32
    ).reshape(tok_rows, -1)
    return (jax.nn.sigmoid(head_gate.astype(jnp.float32)) * attended).astype(jnp.bfloat16)


def on_device(
    hidden,
    query_weight,
    key_weight,
    value_weight,
    head_gate_weight,
    state_in_weight,
    state_gate_weight,
    sink_logit,
    decay_real,
    decay_frequency,
    log_step,
    input_real,
    input_imaginary,
    output_real,
    output_imaginary,
    skip_weight,
    decay_shift,
    head_out_weight,
    state_out_weight,
):
    weight_list = (
        query_weight,
        key_weight,
        value_weight,
        head_gate_weight,
        state_in_weight,
        state_gate_weight,
    )
    portion = gather_hidden(hidden)
    sums = tuple(
        (jnp.dot(portion, weight, preferred_element_type=jnp.float32) for weight in weight_list)
    )
    query_rows_all, key_rows, value_rows, head_gate, state_input, state_gate = tuple(
        (running.astype(jnp.bfloat16) for running in sums)
    )
    key_value = jnp.concatenate([key_rows, value_rows], axis=1)
    head_mixed = attend(query_rows_all, key_value, sink_logit, head_gate)
    state_mixed = recur(
        state_input,
        state_gate,
        decay_real,
        decay_frequency,
        log_step,
        input_real,
        input_imaginary,
        output_real,
        output_imaginary,
        skip_weight,
        decay_shift,
    )
    return project_out(head_mixed, state_mixed, head_out_weight, state_out_weight)


def solution(mesh):
    in_specs = (
        P("sp", "tp"),
        P(None, "tp"),
        P(None, "tp"),
        P(None, "tp"),
        P(None, "tp"),
        P(None, "tp"),
        P(None, "tp"),
        P("tp"),
        P("tp", None),
        P("tp", None),
        P("tp"),
        P("tp", None, None),
        P("tp", None, None),
        P("tp", None, None),
        P("tp", None, None),
        P("tp", None),
        P("tp", "sp"),
        P("tp", None),
        P("tp", None),
    )
    out_specs = P("sp", "tp")
    return jax.shard_map(
        on_device, mesh=mesh, in_specs=in_specs, out_specs=out_specs, check_vma=False
    )
```

time: 355 us -> 171 us (0.48)
  blocking collectives: 158 us -> 0 us
  Pallas kernels: 0 us -> 43.3 us
  local copies, waits for them, and re-layouts: 96.8 us -> 75.9 us
  matrix products: 32.5 us -> 16.9 us
  between operations: 14.6 us -> 0.51 us
  starting transfers between devices: 15.2 us -> 3.11 us
  other arithmetic: 34.7 us -> 30.3 us
    all_gather x6 -> x0, blocking collectives: 158 us -> none  [the longest x4 125 us: carried_in(): gathered = jax.tree.map(lambda a: lax.all_gather(a, axis), part)]
    pallas_call x0 -> x5, Pallas kernels: none -> 43.3 us  [the longest x1 12.6 us: recur(): pl.pallas_call(local_kernel, out_shape=(jax.ShapeDtypeStruct((rows, span)...]
    add x40 -> x1, other arithmetic: 26.6 us -> 0.01 us  [tables(): counter = jnp.arange(1, CHUNK + 1, dtype=F32)[:, None, None]]
    slice x52 -> x0, local copies, waits for them, and re-layouts: 22.2 us -> none  [the longest x43 7.05 us: recur(): inclusive = lax.associative_scan(combine, segment_ends, axis=2)]
    convert_element_type x1 -> x7, local copies, waits for them, and re-layouts: 1.23 us -> 21.1 us  [the longest x3 13.9 us: recur(): uw = (u.astype(F32) * jnp.exp(-relative)).astype(BF16)]
    concatenate x0 -> x5, local copies, waits for them, and re-layouts: none -> 19.7 us  [the longest x4 10.7 us: tables(): stack = lambda a, b: jnp.concatenate([a, b], axis=1)]
    dot_general x8 -> x1, matrix products: 19.8 us -> 0.96 us  [recur(): jnp.dot(decay_shift.reshape(groups * chunks, CHUNK), jnp.asarray(shift_ma...]
    another operation x6 -> x0, local copies, waits for them, and re-layouts: 18.5 us -> none  [the longest x2 6.22 us: recur(): shrink_rows = jnp.tile(jnp.exp(-log_rate), repeats)]
  transfers between devices with their start and end apart: 4 -> 1, of which waited for: 0 -> 0; matrix products, arithmetic and copies ran while one was open for 12% -> 61% of each run, Pallas kernels for 0% -> 18%
where the time goes in v1:
time: 171 us; the launch traced here: 170 us
  local copies, waits for them, and re-layouts  75.9 us (44%)
  Pallas kernels  43.3 us (25%)
  other arithmetic  30.3 us (18%)
  matrix products  16.9 us (10%)
  starting transfers between devices  3.11 us (2%)
    convert_element_type x3, local copies, waits for them, and re-layouts, recur(): uw = (u.astype(F32) * jnp.exp(-relative)).astype(BF16)  13.9 us
    dot_general x6, matrix products, on_device(): jnp.dot(portion, weight, preferred_element_type=jnp.float32)  13.1 us
    pallas_call x1, Pallas kernels, recur(): pl.pallas_call(local_kernel, out_shape=(jax.ShapeDtypeStruct((rows, span)...  12.6 us
    pallas_call x1, Pallas kernels, recur(): pl.pallas_call(carry_kernel, out_shape=jax.ShapeDtypeStruct((groups, stat...  12.5 us
    concatenate x4, local copies, waits for them, and re-layouts, tables(): stack = lambda a, b: jnp.concatenate([a, b], axis=1)  10.7 us
    convert_element_type x3, other arithmetic, halves(): return [high.astype(BF16), (value - high).astype(BF16)]  9.77 us
    reduce_precision x4, local copies, waits for them, and re-layouts, halves(): high = lax.reduce_precision(value, 8, 7)  9.73 us
    concatenate x1, local copies, waits for them, and re-layouts, tables(): jnp.concatenate([h for x in (x1, x2, x3, x4) for h in halves(x)], axis=2)  8.93 us
  transfers between devices with their start and end apart: 1, of which 0 were waited for; matrix products, arithmetic and copies ran while one was open for 61% of the time, Pallas kernels for 18%

profile of v1, /device:TPU:29, one launch (start us, length us, event | category | flops | bytes accessed | tf_op | source)
XLA Modules:
  0.0 170.0 jit_solution(7694875481013852516)
XLA Ops:
  0.0 4.4 %hidden_exchange.1 = bf16[256,2048]{1,0:T(8,128)(2,1)} custom-call(bf16[256,1024]{1,0:T(8,128)(2,1)} %own_ref.1), custom_call_target="tpu_custom_call" | custom-call | tf_op jit(solution)/shard_map/hidden_exchange/pallas_call | solution.py:60
  4.5 2.2 %convolution_convert_fusion.4 = bf16[256,256]{0,1:T(8,128)(2,1)S(1)} fusion(bf16[256,2048]{1,0:T(8,128)(2,1)} %hidden_exchange.1, bf16[2048,256]{1,0:T(8,128)(2,1)} %param.27), kind=kOutput, calls=%fused_computation.29 | convolution fusion | flops 268500992 | bytes 2228224 | tf_op jit(solution)/shard_map/dot_general | solution.py:494
  8.0 3.1 %collective-permute-start = (bf16[128,512]{0,1:T(8,128)(2,1)}, bf16[128,512]{0,1:T(8,128)(2,1)}, u32[]{:S(2)}, u32[]{:S(2)}) collective-permute-start(bf16[128,512]{0,1:T(8,128)(2,1)} %fusion.37), channel_id=1, source_target_pairs={{0,2},{2,4},{4,6},{6,8},{8,10},{10,12},{12,14},{14,16},{16,18},{18... | collective-permute-start | bytes 393224 | tf_op jit(solution)/shard_map/ppermute | solution.py:29
  14.1 2.0 %copy.78 = f32[32,128,16]{2,1,0:T(8,128)} copy(f32[32,128,16]{1,2,0:T(8,128)S(1)} %get-tuple-element.30) | data formatting | bytes 524288 | tf_op jit(solution)/shard_map/concatenate | solution.py:320
  16.1 2.9 %copy.74 = f32[32,128,16]{2,1,0:T(8,128)} copy(f32[32,128,16]{1,2,0:T(8,128)} %get-tuple-element.46) | data formatting | bytes 524288 | tf_op jit(solution)/shard_map/concatenate | solution.py:320
  23.4 2.9 %copy.79 = f32[32,128,16]{2,1,0:T(8,128)} copy(f32[32,128,16]{1,2,0:T(8,128)} %get-tuple-element.29) | data formatting | bytes 524288 | tf_op jit(solution)/shard_map/reduce_precision | solution.py:294
  27.2 2.9 %copy.80 = f32[32,128,16]{2,1,0:T(8,128)} copy(f32[32,128,16]{1,2,0:T(8,128)} %get-tuple-element.44) | data formatting | bytes 524288 | tf_op jit(solution)/shard_map/concatenate | solution.py:320
  30.1 2.9 %copy.81 = f32[32,128,16]{2,1,0:T(8,128)} copy(f32[32,128,16]{1,2,0:T(8,128)} %get-tuple-element.42) | data formatting | bytes 524288 | tf_op jit(solution)/shard_map/reduce_precision | solution.py:294
  33.0 2.0 %copy.75 = f32[32,128,16]{2,1,0:T(8,128)} copy(f32[32,128,16]{1,2,0:T(8,128)S(1)} %copy-done.10) | data formatting | bytes 524288 | tf_op jit(solution)/shard_map/reduce_precision | solution.py:294
  35.0 1.9 %fusion.55 = (f32[32,128,16]{1,2,0:T(8,128)S(1)}, bf16[32,128,16]{1,2,0:T(8,128)(2,1)}, f32[32,128,16]{1,2,0:T(8,128)}) fusion(f32[32,64,16]{1,2,0:T(8,128)} %bitcast.59), kind=kLoop, calls=%fused_computation.159 | loop fusion | flops 196608 | bytes 786432 | tf_op jit(solution)/shard_map/reduce_precision | solution.py:294
  36.9 2.9 %copy.76 = f32[32,128,16]{2,1,0:T(8,128)} copy(f32[32,128,16]{1,2,0:T(8,128)} %get-tuple-element.49) | data formatting | bytes 524288 | tf_op jit(solution)/shard_map/concatenate | solution.py:320
  39.8 2.0 %copy.77 = f32[32,128,16]{2,1,0:T(8,128)} copy(f32[32,128,16]{1,2,0:T(8,128)S(1)} %get-tuple-element.47) | data formatting | bytes 524288 | tf_op jit(solution)/shard_map/reduce_precision | solution.py:294
  41.9 2.3 %copy.82 = bf16[32,128,16]{2,1,0:T(8,128)(2,1)} copy(bf16[32,128,16]{1,2,0:T(8,128)(2,1)} %get-tuple-element.71) | data formatting | bytes 262144 | tf_op jit(solution)/shard_map/convert_element_type | solution.py:295
  44.1 2.2 %copy.84 = bf16[32,128,16]{2,1,0:T(8,128)(2,1)} copy(bf16[32,128,16]{1,2,0:T(8,128)(2,1)} %get-tuple-element.70) | data formatting | bytes 262144 | tf_op jit(solution)/shard_map/convert_element_type | solution.py:295
  58.5 3.8 %reshape.162 = f32[16,16,32,16]{3,2,1,0:T(8,128)} reshape(f32[256,512]{1,0:T(8,128)} %fusion.15) | data formatting | bytes 1048576 | tf_op jit(solution)/shard_map/convert_element_type | solution.py:378
  62.2 6.6 %copy.72 = f32[32,16,16,16]{3,2,1,0:T(8,128)} copy(f32[32,16,16,16]{3,0,2,1:T(8,128)} %bitcast.56) | data formatting | bytes 1048576 | tf_op jit(solution)/shard_map/convert_element_type | solution.py:378
  68.9 3.5 %reshape.161 = f32[512,256]{1,0:T(8,128)S(1)} reshape(f32[32,16,16,16]{3,2,1,0:T(8,128)} %copy.72) | data formatting | bytes 1048576 | tf_op jit(solution)/shard_map/convert_element_type | solution.py:378
  76.9 5.9 %subtract_convert_fusion = (bf16[32,128,16]{2,1,0:T(8,128)(2,1)}, bf16[32,128,16]{2,1,0:T(8,128)(2,1)}) fusion(f32[32,128,16]{2,1,0:T(8,128)} %copy.80, f32[32,128,16]{2,1,0:T(8,128)} %copy.81, f32[32,128,16]{2,1,0:T(8,128)} %copy.78, f32[32,128,16]{2,1,0:T(8,128)} %copy.79), kind=kLoop, calls=%fused_computation.1 | loop fusion | flops 262144 | bytes 1310720 | tf_op jit(solution)/shard_map/convert_element_type | solution.py:295
  83.6 2.2 %subtract_convert_fusion.2 = (bf16[32,128,16]{2,1,0:T(8,128)(2,1)}, bf16[32,128,16]{2,1,0:T(8,128)(2,1)}) fusion(f32[32,128,16]{2,1,0:T(8,128)S(1)} %copy-done.5, f32[32,128,16]{2,1,0:T(8,128)S(1)} %copy-done.6, f32[32,128,16]{2,1,0:T(8,128)S(1)} %copy-done.3, f32[32,128,16]{2,1,0:T(8,128)S(1)} %copy-done.4), kind=kLoop, calls=%fused_computation.3 | loop fusion | flops 262144 | bytes 1310720 | tf_op jit(solution)/shard_map/convert_element_type | solution.py:295
  85.7 8.9 %concatenate.60.gtab_ref = bf16[32,128,128]{2,1,0:T(8,128)(2,1)} concatenate(bf16[32,128,16]{2,1,0:T(8,128)(2,1)} %copy.82, bf16[32,128,16]{2,1,0:T(8,128)(2,1)} %get-tuple-element.75, bf16[32,128,16]{2,1,0:T(8,128)(2,1)} %copy.83, bf16[32,128,16]{2,1,0:T(8,128)(2,1)} %get-tuple-element.74, bf16[32,128,16]{2,1,0:T(8,128)(2,1)} %copy.84, bf16[32,128,16]{2,1,0:T(8,128)(2,1)} %get-tuple-element.73, ...), dimensions={2} | concatenate | bytes 2097152 | tf_op jit(solution)/shard_map/concatenate | solution.py:325
  94.7 12.6 %state_local.1 = (f32[512,256]{1,0:T(8,128)}, bf16[32,128,256]{2,1,0:T(8,128)(2,1)}, f32[512,128]{1,0:T(8,128)}, f32[40,128]{1,0:T(8,128)}) custom-call(bf16[512,256]{1,0:T(8,128)(2,1)} %get-tuple-element.37.uw_ref, bf16[32,128,128]{2,1,0:T(8,128)(2,1)} %concatenate.60.gtab_ref, bf16[32,128,128]{2,1,0:T(8,128)(2,1)} %copy-done.7, ...), custom_call_target="tpu_custom_call" | custom-call | tf_op jit(solution)/shard_map/state_local/pallas_call | solution.py:381
  107.2 12.5 %state_carry.1.carry_ref = f32[32,128]{1,0:T(8,128)} custom-call(f32[40,128]{1,0:T(8,128)} %get-tuple-element.21.msg_ref, f32[32,128]{1,0:T(8,128)} %get-tuple-element.76.same_ref, f32[32,128]{1,0:T(8,128)} %get-tuple-element.77.swapped_ref), custom_call_target="tpu_custom_call" | custom-call | tf_op jit(solution)/shard_map/state_carry/pallas_call | solution.py:395
  119.8 4.9 %state_finish.1 = f32[512,256]{1,0:T(8,128)} custom-call(f32[32,128]{1,0:T(8,128)} %state_carry.1.carry_ref, f32[512,128]{1,0:T(8,128)} %get-tuple-element.22.pushed_ref, f32[512,256]{1,0:T(8,128)} %get-tuple-element.23.intra_ref, bf16[32,128,256]{2,1,0:T(8,128)(2,1)} %get-tuple-element.24.g_ref, f32[512,256]{1,0:T(8,128)} %get-tuple-element.36.wout_ref, ...), custom_call_target="tpu_custom_call" | custom-call | tf_op jit(solution)/shard_map/state_finish/pallas_call | solution.py:408
  124.7 3.7 %reshape.159 = f32[32,16,16,16]{3,2,1,0:T(8,128)} reshape(f32[512,256]{1,0:T(8,128)} %state_finish.1) | data formatting | bytes 1048576 | tf_op jit(solution)/shard_map/reshape | solution.py:418
  128.4 6.6 %copy.86 = f32[16,16,32,16]{3,2,1,0:T(8,128)} copy(f32[16,16,32,16]{3,1,0,2:T(8,128)} %bitcast.55) | data formatting | bytes 1048576 | tf_op jit(solution)/shard_map/transpose | solution.py:419
  135.1 4.5 %reshape.160 = f32[256,512]{1,0:T(8,128)S(1)} reshape(f32[16,16,32,16]{3,2,1,0:T(8,128)} %copy.86) | data formatting | bytes 1048576 | tf_op jit(solution)/shard_map/reshape | solution.py:420
  139.8 2.4 %convolution_convert_fusion.2 = bf16[256,512]{1,0:T(8,128)(2,1)S(1)} fusion(bf16[256,2048]{1,0:T(8,128)(2,1)S(1)} %copy-done.2, bf16[2048,512]{1,0:T(8,128)(2,1)} %param.25), kind=kOutput, calls=%fused_computation.12 | convolution fusion | flops 537001984 | bytes 3407872 | tf_op jit(solution)/shard_map/dot_general | solution.py:494
  143.5 3.2 %fusion.14.state_ref = bf16[256,512]{1,0:T(8,128)(2,1)} fusion(bf16[256,2048]{1,0:T(8,128)(2,1)S(1)} %copy-done.2, bf16[2048,512]{1,0:T(8,128)(2,1)} %param.30, f32[256,512]{1,0:T(8,128)S(1)} %reshape.160, f32[256,512]{1,0:T(8,128)S(1)} %copy-done.12, f32[512]{0:T(512)S(1)} %mul.494), kind=kOutput, calls=%fused_computation.27 | convolution fusion | flops 539099136 | bytes 4458496 | tf_op jit(solution)/shard_map/dot_general | solution.py:494
  152.3 1.9 %copy.94 = f32[2,128,4,2,64]{4,3,2,1,0:T(2,128)S(1)} copy(f32[2,128,4,2,64]{1,4,3,2,0:T(8,128)} %convolution_bitcast_fusion.1) | data formatting | bytes 1048576 | tf_op jit(solution)/shard_map/reshape | solution.py:459
  155.9 3.3 %fusion.7.head_ref = bf16[256,512]{1,0:T(8,128)(2,1)} fusion(f32[256,512]{1,0:T(8,128)} %reshape.166, bf16[256,2048]{1,0:T(8,128)(2,1)S(1)} %copy-done.2, bf16[2048,512]{1,0:T(8,128)(2,1)} %param.28), kind=kOutput, calls=%fused_computation.20 | convolution fusion | flops 537788416 | bytes 3932160 | tf_op jit(solution)/shard_map/dot_general | solution.py:494
  159.2 8.8 %output_projection.1 = bf16[256,1024]{1,0:T(8,128)(2,1)} custom-call(bf16[256,512]{1,0:T(8,128)(2,1)} %fusion.7.head_ref, bf16[256,512]{1,0:T(8,128)(2,1)} %fusion.14.state_ref, bf16[512,2048]{1,0:T(8,128)(2,1)} %how_ref.1, bf16[512,2048]{1,0:T(8,128)(2,1)} %sow_ref.1), custom_call_target="tpu_custom_call" | custom-call | tf_op jit(solution)/shard_map/output_projection/pallas_call | solution.py:114
  168.1 1.9 %copy.109 = bf16[256,1024]{1,0:T(8,128)(2,1)} copy(bf16[256,1024]{1,0:T(8,128)(2,1)} %output_projection.1) | data formatting | bytes 1048576
  (118 shorter events, 35.5 us)
Async XLA Ops:
  0.0 57.0 %copy-start = (bf16[2048,512]{1,0:T(8,128)(2,1)S(1)}, bf16[2048,512]{1,0:T(8,128)(2,1)}, u32[]{:S(2)}) copy-start(bf16[2048,512]{1,0:T(8,128)(2,1)} %param.29) | copy-start | bytes 6291460
  4.4 2.3 %copy-start.2 = (bf16[256,2048]{1,0:T(8,128)(2,1)S(1)}, bf16[256,2048]{1,0:T(8,128)(2,1)}, u32[]{:S(2)}) copy-start(bf16[256,2048]{1,0:T(8,128)(2,1)} %hidden_exchange.1) | copy-start | bytes 3145732
  4.4 2.3 %copy-start.11 = (bf16[2048,256]{1,0:T(8,128)(2,1)S(1)}, bf16[2048,256]{1,0:T(8,128)(2,1)}, u32[]{:S(2)}) copy-start(bf16[2048,256]{1,0:T(8,128)(2,1)} %param.26) | copy-start | bytes 3145732
  4.4 6.6 %copy-start.29 = (f32[32]{0:T(128)S(1)}, f32[32]{0:T(128)}, u32[]{:S(2)}) copy-start(f32[32]{0:T(128)} %param.34) | copy-start | bytes 388
  4.5 6.7 %copy-start.23 = (f32[32,64]{1,0:T(8,128)S(1)}, f32[32,64]{1,0:T(8,128)}, u32[]{:S(2)}) copy-start(f32[32,64]{1,0:T(8,128)} %param.33) | copy-start | bytes 24580
  4.5 6.7 %copy-start.24 = (f32[32,64]{1,0:T(8,128)S(1)}, f32[32,64]{1,0:T(8,128)}, u32[]{:S(2)}) copy-start(f32[32,64]{1,0:T(8,128)} %param.32) | copy-start | bytes 24580
  7.3 5.7 %copy-start.8 = (bf16[256,256]{0,1:T(8,128)(2,1)}, bf16[256,256]{0,1:T(8,128)(2,1)S(1)}, u32[]{:S(2)}) copy-start(bf16[256,256]{0,1:T(8,128)(2,1)S(1)} %convolution_convert_fusion.5) | copy-start | bytes 393220
  8.0 138.8 %collective-permute-start = (bf16[128,512]{0,1:T(8,128)(2,1)}, bf16[128,512]{0,1:T(8,128)(2,1)}, u32[]{:S(2)}, u32[]{:S(2)}) collective-permute-start(bf16[128,512]{0,1:T(8,128)(2,1)} %fusion.37), channel_id=1, source_target_pairs={{0,2},{2,4},{4,6},{6,8},{8,10},{10,12},{12,14},{14,16},{16,18},{18... | collective-permute-start | bytes 393224 | tf_op jit(solution)/shard_map/ppermute | solution.py:29
  11.1 1.9 %copy-start.26 = (f32[16]{0:T(128)}, f32[16]{0:T(128)S(1)}, u32[]{:S(2)}) copy-start(f32[16]{0:T(128)S(1)} %iota_add_fusion) | copy-start | bytes 196
  11.9 1.1 copy-start.16
  20.6 5.6 %copy-start.15 = (f32[32,16,64]{2,1,0:T(8,128)S(1)}, f32[32,16,64]{2,1,0:T(8,128)}, u32[]{:S(2)}) copy-start(f32[32,16,64]{2,1,0:T(8,128)} %param.38) | copy-start | bytes 393220
  27.2 5.8 %copy-start.10 = (f32[32,128,16]{1,2,0:T(8,128)S(1)}, f32[32,128,16]{1,2,0:T(8,128)}, u32[]{:S(2)}) copy-start(f32[32,128,16]{1,2,0:T(8,128)} %get-tuple-element.45) | copy-start | bytes 786436
  41.9 4.5 %copy-start.14 = (bf16[32,128,16]{1,2,0:T(8,128)(2,1)S(1)}, bf16[32,128,16]{1,2,0:T(8,128)(2,1)}, u32[]{:S(2)}) copy-start(bf16[32,128,16]{1,2,0:T(8,128)(2,1)} %get-tuple-element.48) | copy-start | bytes 393220
  41.9 5.9 %copy-start.13 = (bf16[32,128,16]{1,2,0:T(8,128)(2,1)S(1)}, bf16[32,128,16]{1,2,0:T(8,128)(2,1)}, u32[]{:S(2)}) copy-start(bf16[32,128,16]{1,2,0:T(8,128)(2,1)} %get-tuple-element.43) | copy-start | bytes 393220
  47.7 3.4 %copy-start.18 = (f32[32,64]{1,0:T(8,128)S(1)}, f32[32,64]{1,0:T(8,128)}, u32[]{:S(2)}) copy-start(f32[32,64]{1,0:T(8,128)} %get-tuple-element.55) | copy-start | bytes 24580
  47.7 3.4 %copy-start.19 = (f32[32,64]{1,0:T(8,128)S(1)}, f32[32,64]{1,0:T(8,128)}, u32[]{:S(2)}) copy-start(f32[32,64]{1,0:T(8,128)} %get-tuple-element.56) | copy-start | bytes 24580
  53.2 1.0 copy-start.7
  68.9 3.5 %copy-start.17 = (f32[32,256]{1,0:T(8,128)S(1)}, f32[32,256]{1,0:T(8,128)}, u32[]{:S(2)}) copy-start(f32[32,256]{1,0:T(8,128)} %param.40) | copy-start | bytes 98308
  68.9 3.6 %copy-start.22 = (f32[16,512]{1,0:T(8,128)S(1)}, f32[16,512]{1,0:T(8,128)}, u32[]{:S(2)}) copy-start(f32[16,512]{1,0:T(8,128)} %constant.69.clone) | copy-start | bytes 98308
  72.5 3.6 %copy-start.20 = (f32[32,64]{1,0:T(8,128)S(1)}, f32[32,64]{1,0:T(8,128)}, u32[]{:S(2)}) copy-start(f32[32,64]{1,0:T(8,128)} %get-tuple-element.26) | copy-start | bytes 24580
  72.6 3.6 %copy-start.21 = (f32[32,64]{1,0:T(8,128)S(1)}, f32[32,64]{1,0:T(8,128)}, u32[]{:S(2)}) copy-start(f32[32,64]{1,0:T(8,128)} %get-tuple-element.62) | copy-start | bytes 24580
  76.9 5.9 %copy-start.3 = (f32[32,128,16]{2,1,0:T(8,128)S(1)}, f32[32,128,16]{2,1,0:T(8,128)}, u32[]{:S(2)}) copy-start(f32[32,128,16]{2,1,0:T(8,128)} %copy.74) | copy-start | bytes 786436
  76.9 5.9 %copy-start.4 = (f32[32,128,16]{2,1,0:T(8,128)S(1)}, f32[32,128,16]{2,1,0:T(8,128)}, u32[]{:S(2)}) copy-start(f32[32,128,16]{2,1,0:T(8,128)} %copy.75) | copy-start | bytes 786436
  76.9 5.9 %copy-start.5 = (f32[32,128,16]{2,1,0:T(8,128)S(1)}, f32[32,128,16]{2,1,0:T(8,128)}, u32[]{:S(2)}) copy-start(f32[32,128,16]{2,1,0:T(8,128)} %copy.76) | copy-start | bytes 786436
  76.9 6.7 %copy-start.6 = (f32[32,128,16]{2,1,0:T(8,128)S(1)}, f32[32,128,16]{2,1,0:T(8,128)}, u32[]{:S(2)}) copy-start(f32[32,128,16]{2,1,0:T(8,128)} %copy.77) | copy-start | bytes 786436
  135.1 4.5 %copy-start.25 = (f32[32,16]{0,1:T(8,128)S(1)}, f32[32,16]{0,1:T(8,128)}, u32[]{:S(2)}) copy-start(f32[32,16]{0,1:T(8,128)} %param.39) | copy-start | bytes 6148
  139.8 3.5 %copy-start.27 = (s32[128]{0:T(128)S(1)}, s32[128]{0:T(128)}, u32[]{:S(2)}) copy-start(s32[128]{0:T(128)} %iota_add_fusion.1) | copy-start | bytes 1540
  139.8 3.6 %copy-start.28 = (f32[8]{0:T(128)S(1)}, f32[8]{0:T(128)}, u32[]{:S(2)}) copy-start(f32[8]{0:T(128)} %param.31) | copy-start | bytes 100
  139.8 3.7 %copy-start.12 = (f32[256,512]{1,0:T(8,128)S(1)}, f32[256,512]{1,0:T(8,128)}, u32[]{:S(2)}) copy-start(f32[256,512]{1,0:T(8,128)} %fusion.15) | copy-start | bytes 1572868
  143.5 3.4 %copy-start.9 = (bf16[256,256]{0,1:T(8,128)(2,1)S(1)}, bf16[256,256]{0,1:T(8,128)(2,1)}, u32[]{:S(2)}) copy-start(bf16[256,256]{0,1:T(8,128)(2,1)} %copy-done.8) | copy-start | bytes 393220
  155.9 14.0 %copy-start.1 = (bf16[2048,512]{1,0:T(8,128)(2,1)S(1)}, bf16[2048,512]{1,0:T(8,128)(2,1)}, u32[]{:S(2)}) copy-start(bf16[2048,512]{1,0:T(8,128)(2,1)} %param.29) | copy-start | bytes 6291460

commit v2 on v1

v2 whole, which is shorter than its diff:
```python
import jax
import jax.numpy as jnp
import numpy as np
from jax import lax
from jax.experimental import pallas as pl
from jax.experimental.pallas import tpu as pltpu
from jax.sharding import PartitionSpec as P

HEAD_DIM = 64
Q_HEADS = 16
KV_HEADS = 8
GROUP_CH = 16
WINDOW = 128
CHUNK = 16
LANES = 128

NEG_FILL = -1e30
MESH = pl.DeviceIdType.MESH
VMEM = pl.BlockSpec(memory_space=pltpu.VMEM)
BF16 = jnp.bfloat16
F32 = jnp.float32


def params(collective_id=None):
    extra = {} if collective_id is None else {"collective_id": collective_id, "has_side_effects": True}
    return pltpu.CompilerParams(vmem_limit_bytes=60 * 1024 * 1024, **extra)


def hidden_kernel(own_ref, full_ref, send_sem, recv_sem):
    me = lax.axis_index("tp")
    other = 1 - me
    width = own_ref.shape[1]
    barrier = pltpu.get_barrier_semaphore()
    pl.semaphore_signal(barrier, inc=1, device_id={"tp": other}, device_id_type=MESH)
    pl.semaphore_wait(barrier, 1)
    mine = pl.ds(pl.multiple_of(me * width, LANES), width)
    copy = pltpu.make_async_remote_copy(
        src_ref=own_ref,
        dst_ref=full_ref.at[:, mine],
        send_sem=send_sem,
        recv_sem=recv_sem,
        device_id={"tp": other},
        device_id_type=MESH,
    )
    copy.start()
    full_ref[:, mine] = own_ref[...]
    copy.wait()


def gather_hidden(hidden):
    rows, width = hidden.shape
    return pl.pallas_call(
        hidden_kernel,
        out_shape=jax.ShapeDtypeStruct((rows, 2 * width), hidden.dtype),
        in_specs=[VMEM],
        out_specs=VMEM,
        scratch_shapes=[pltpu.SemaphoreType.DMA, pltpu.SemaphoreType.DMA],
        compiler_params=params(0),
        name="hidden_exchange",
    )(hidden)


def output_kernel(head_ref, state_ref, how_ref, sow_ref, out_ref, away, landed, send_sem, recv_sem):
    me = lax.axis_index("tp")
    other = 1 - me
    rows, width = out_ref.shape
    pieces = away.shape[0]
    step = width // pieces
    barrier = pltpu.get_barrier_semaphore()
    pl.semaphore_signal(barrier, inc=1, device_id={"tp": other}, device_id_type=MESH)
    pl.semaphore_wait(barrier, 1)

    def product(owner, piece):
        columns = pl.ds(pl.multiple_of(owner * width + piece * step, LANES), step)
        return jnp.dot(head_ref[...], how_ref[:, columns], preferred_element_type=F32) + jnp.dot(
            state_ref[...], sow_ref[:, columns], preferred_element_type=F32
        )

    copies = [
        pltpu.make_async_remote_copy(
            src_ref=away.at[piece],
            dst_ref=landed.at[piece],
            send_sem=send_sem.at[piece],
            recv_sem=recv_sem.at[piece],
            device_id={"tp": other},
            device_id_type=MESH,
        )
        for piece in range(pieces)
    ]
    for piece in range(pieces):
        away[piece] = product(other, piece).astype(away.dtype)
        if piece > 0:
            copies[piece - 1].start()
    own = [product(me, 0)]
    copies[pieces - 1].start()
    for piece in range(pieces):
        total = own[0] if piece == 0 else product(me, piece)
        copies[piece].wait()
        out_ref[:, pl.ds(piece * step, step)] = (total + landed[piece].astype(F32)).astype(out_ref.dtype)


def project_out(head_mixed, state_mixed, head_out_weight, state_out_weight):
    rows = head_mixed.shape[0]
    width = head_out_weight.shape[1] // 2
    pieces = 4
    return pl.pallas_call(
        output_kernel,
        out_shape=jax.ShapeDtypeStruct((rows, width), BF16),
        in_specs=[VMEM] * 4,
        out_specs=VMEM,
        scratch_shapes=[
            pltpu.VMEM((pieces, rows, width // pieces), F32),
            pltpu.VMEM((pieces, rows, width // pieces), F32),
            pltpu.SemaphoreType.DMA((pieces,)),
            pltpu.SemaphoreType.DMA((pieces,)),
        ],
        compiler_params=params(1),
        name="output_projection",
    )(head_mixed, state_mixed, head_out_weight, state_out_weight)


def turn(value, same, swapped):
    return value * same + pltpu.roll(value, value.shape[1] // 2, 1) * swapped


def regroup(parts):
    block = lax.broadcasted_iota(jnp.int32, parts[0].shape, 1) // GROUP_CH
    parts = list(parts)
    for distance in (4, 2, 1):
        low = (block & distance) == 0
        amount = distance * GROUP_CH
        for i in range(len(parts)):
            if i & distance:
                continue
            first, second = parts[i], parts[i + distance]
            parts[i] = jnp.where(low, first, pltpu.roll(second, amount, 1))
            parts[i + distance] = jnp.where(low, pltpu.roll(first, LANES - amount, 1), second)
    return parts


def split(value):
    high = value.astype(BF16)
    return [high, (value - high.astype(F32)).astype(BF16)]


def local_kernel(
    state_ref, win_ref, x1g_ref, x3g_ref, x1d_ref, x3d_ref, inr_ref, ini_ref, outr_ref, outi_ref,
    zr_ref, zi_ref, et_ref, a16_ref, b16_ref, tail_ref, whole_ref, tile_ref,
    intra_ref, g_ref, pushed_ref, msg_ref, wide, uw,
):
    groups = zr_ref.shape[0]
    chunks = win_ref.shape[0] // groups
    span = win_ref.shape[1]
    per_tile = LANES // GROUP_CH
    for tile in range(groups // per_tile):
        wide[tile] = state_ref[:, pl.ds(tile * LANES, LANES)].astype(F32)
        for half in range(span // LANES):
            parts = regroup([
                wide[tile, pl.ds(half * per_tile + k, chunks, stride=CHUNK), :] for k in range(per_tile)
            ])
            for k in range(per_tile):
                rows = pl.ds((tile * per_tile + k) * chunks, chunks)
                columns = pl.ds(half * LANES, LANES)
                uw[rows, columns] = (parts[k] * win_ref[rows, columns]).astype(BF16)
    row = lax.broadcasted_iota(jnp.int32, (span, span), 0) // GROUP_CH
    column = lax.broadcasted_iota(jnp.int32, (span, span), 1) // GROUP_CH
    causal = row <= column
    batch = 4
    beside = lambda a, b: jnp.concatenate([a, b], axis=1)

    def table_of(g):
        one_row = pl.ds(g, 1)
        drive_in = beside(inr_ref[g], ini_ref[g])
        x2d = zr_ref[one_row, :] * drive_in + zi_ref[one_row, :] * beside(ini_ref[g], inr_ref[g])
        x4d = pltpu.roll(x2d, LANES // 2, 1)
        x2g = beside(outr_ref[g], outr_ref[g])
        x4g = beside(outi_ref[g], outi_ref[g])
        stack = lambda xs: jnp.concatenate([h for x in xs for h in split(x)], axis=0)
        return beside(
            stack([x1g_ref[g], x2g, x3g_ref[g], x4g]), stack([x1d_ref[g], x2d, x3d_ref[g], x4d])
        )

    def one(step, carry):
        ids = [step * batch + k for k in range(batch)]
        tall = [jnp.dot(et_ref[...], table_of(g), preferred_element_type=F32) for g in ids]
        both = [
            (x[:span] * x[span : 2 * span] + x[2 * span : 3 * span] * x[3 * span :]).astype(BF16)
            for x in tall
        ]
        out_side = [x[:, :LANES] for x in both]
        in_side = [x[:, LANES:] for x in both]
        for g, value in zip(ids, out_side):
            g_ref[g] = value
        table = [
            jnp.where(
                causal,
                lax.dot_general(a, b, (((1,), (1,)), ((), ())), preferred_element_type=F32),
                0.0,
            ).astype(BF16)
            for a, b in zip(in_side, out_side)
        ]
        for g, t, d in zip(ids, table, in_side):
            rows = pl.ds(pl.multiple_of(g * chunks, chunks), chunks)
            u = uw[rows, :]
            intra_ref[rows, :] = jnp.dot(u, t, preferred_element_type=F32)
            pushed_ref[rows, :] = jnp.dot(u, d, preferred_element_type=F32)
        return carry

    lax.fori_loop(0, groups // batch, one, 0)
    same, swapped = a16_ref[...], b16_ref[...]
    state = jnp.zeros((groups, pushed_ref.shape[1]), F32)
    for c in range(chunks):
        rows = pl.ds(c, groups, stride=chunks)
        local = tail_ref[rows, :] * turn(pushed_ref[rows, :], same, swapped)
        pushed_ref[rows, :] = local
        state = whole_ref[rows, :] * turn(state, same, swapped) + local
    msg_ref[:groups, :] = state
    msg_ref[groups:, :] = tile_ref[...]


def attend_block(block, first_device, query_ref, gate_ref, sink_ref, keys, values, head_ref):
    rows = pl.ds(block * WINDOW, WINDOW)
    band = pl.ds(block * WINDOW, 2 * WINDOW)
    query_index = lax.broadcasted_iota(jnp.int32, (WINDOW, 2 * WINDOW), 0)
    column = lax.broadcasted_iota(jnp.int32, (WINDOW, 2 * WINDOW), 1)
    distance = WINDOW + query_index - column
    allowed = (distance >= 0) & (distance < WINDOW)
    if block == 0:
        allowed = allowed & (column >= jnp.where(first_device, WINDOW, 0))
    group_size = Q_HEADS // KV_HEADS
    heads = query_ref.shape[1] // HEAD_DIM
    query, key, value = query_ref[rows, :], keys[band, :], values[band, :]
    gate = gate_ref[rows, :].astype(F32)
    results = []
    for head in range(heads):
        kv = head // group_size
        q = query[:, head * HEAD_DIM : (head + 1) * HEAD_DIM]
        k = key[:, kv * HEAD_DIM : (kv + 1) * HEAD_DIM]
        v = value[:, kv * HEAD_DIM : (kv + 1) * HEAD_DIM]
        scores = lax.dot_general(q, k, (((1,), (1,)), ((), ())), preferred_element_type=F32)
        scores = jnp.where(allowed, scores * HEAD_DIM ** (-0.5), NEG_FILL)
        sink = sink_ref[head]
        maxima = jnp.maximum(jnp.max(scores, axis=-1, keepdims=True), sink)
        exponent = jnp.exp(scores - maxima)
        totals = jnp.sum(exponent, axis=-1, keepdims=True) + jnp.exp(sink - maxima)
        weights = (exponent * (1.0 / totals)).astype(BF16)
        results.append(jnp.dot(weights, v, preferred_element_type=F32))
    attended = jnp.concatenate(results, axis=1)
    head_ref[rows, :] = (jax.nn.sigmoid(gate) * attended).astype(head_ref.dtype)


def carry_kernel(
    msg_ref, same_ref, swapped_ref, query_ref, key_ref, value_ref, gate_ref, sink_ref,
    carry_ref, head_ref, landed, keys, values, send_sem, recv_sem, halo_send, halo_recv,
):
    me = lax.axis_index("sp")
    count = lax.axis_size("sp")
    groups = carry_ref.shape[0]
    tok_rows = key_ref.shape[0]
    barrier = pltpu.get_barrier_semaphore()

    def greet(hop, x):
        pl.semaphore_signal(
            barrier, inc=1, device_id={"sp": lax.rem(me + hop, count)}, device_id_type=MESH
        )
        return x

    lax.fori_loop(1, count, greet, 0)
    pl.semaphore_wait(barrier, count - 1)

    def outgoing(target):
        return pltpu.make_async_remote_copy(
            src_ref=msg_ref,
            dst_ref=landed.at[me],
            send_sem=send_sem.at[target],
            recv_sem=recv_sem.at[me],
            device_id={"sp": target},
            device_id_type=MESH,
        )

    def incoming(source):
        return pltpu.make_async_remote_copy(
            src_ref=msg_ref,
            dst_ref=landed.at[source],
            send_sem=send_sem.at[source],
            recv_sem=recv_sem.at[source],
            device_id={"sp": source},
            device_id_type=MESH,
        )

    def halos(target):
        return [
            pltpu.make_async_remote_copy(
                src_ref=own.at[pl.ds(tok_rows - WINDOW, WINDOW)],
                dst_ref=band.at[pl.ds(0, WINDOW)],
                send_sem=halo_send.at[k],
                recv_sem=halo_recv.at[k],
                device_id={"sp": target},
                device_id_type=MESH,
            )
            for k, (own, band) in enumerate(((key_ref, keys), (value_ref, values)))
        ]

    @pl.when(me < count - 1)
    def _():
        for copy in halos(me + 1):
            copy.start()

    def send(target, x):
        outgoing(target).start()
        return x

    lax.fori_loop(me + 1, count, send, 0)
    own_rows = pl.ds(WINDOW, tok_rows)
    keys[own_rows, :] = key_ref[...]
    values[own_rows, :] = value_ref[...]

    @pl.when(me == 0)
    def _():
        keys[:WINDOW, :] = jnp.zeros((WINDOW, keys.shape[1]), keys.dtype)
        values[:WINDOW, :] = jnp.zeros((WINDOW, values.shape[1]), values.dtype)

    blocks = tok_rows // WINDOW
    for block in range(1, blocks):
        attend_block(block, me == 0, query_ref, gate_ref, sink_ref, keys, values, head_ref)

    @pl.when(me > 0)
    def _():
        for copy in halos(me):
            copy.wait_recv()

    attend_block(0, me == 0, query_ref, gate_ref, sink_ref, keys, values, head_ref)

    same, swapped = same_ref[...], swapped_ref[...]
    pick = lax.broadcasted_iota(jnp.int32, (groups, LANES), 0) == lax.broadcasted_iota(
        jnp.int32, (groups, LANES), 1
    )

    def absorb(source, state):
        incoming(source).wait_recv()
        shift_row = landed[source, pl.ds(groups, 1), :]
        total = jnp.sum(jnp.where(pick, shift_row, 0.0), axis=1, keepdims=True)
        return jnp.exp(total) * turn(state, same, swapped) + landed[source, pl.ds(0, groups), :]

    carry_ref[...] = lax.fori_loop(0, me, absorb, jnp.zeros(carry_ref.shape, F32))

    def drain(target, x):
        outgoing(target).wait_send()
        return x

    lax.fori_loop(me + 1, count, drain, 0)

    @pl.when(me < count - 1)
    def _():
        for copy in halos(me + 1):
            copy.wait_send()


def finish_kernel(
    carry_ref, pushed_ref, intra_ref, g_ref, wout_ref, a16_ref, b16_ref, head_ref, whole_ref,
    state_ref, gate_ref, skip_ref, mixed_ref, entry, grouped, rows_out,
):
    groups = g_ref.shape[0]
    chunks = pushed_ref.shape[0] // groups
    span = intra_ref.shape[1]
    per_tile = LANES // GROUP_CH
    same, swapped = a16_ref[...], b16_ref[...]
    state = carry_ref[...]
    for c in range(chunks):
        rows = pl.ds(c, groups, stride=chunks)
        entry[rows, :] = head_ref[rows, :] * state
        state = whole_ref[rows, :] * turn(state, same, swapped) + pushed_ref[rows, :]
    batch = 8

    def one(step, x):
        for k in range(batch):
            g = step * batch + k
            rows = pl.ds(pl.multiple_of(g * chunks, chunks), chunks)
            far = lax.dot_general(
                entry[rows, :].astype(BF16), g_ref[g], (((1,), (1,)), ((), ())),
                preferred_element_type=F32,
            )
            grouped[rows, :] = wout_ref[rows, :] * (intra_ref[rows, :] + far)
        return x

    lax.fori_loop(0, groups // batch, one, 0)
    for tile in range(groups // per_tile):
        lanes = pl.ds(tile * LANES, LANES)
        for half in range(span // LANES):
            columns = pl.ds(half * LANES, LANES)
            parts = regroup([
                grouped[pl.ds((tile * per_tile + k) * chunks, chunks), columns]
                for k in range(per_tile)
            ])
            for k in range(per_tile):
                rows_out[tile, pl.ds(half * per_tile + k, chunks, stride=CHUNK), :] = parts[k]
        recurrent = rows_out[tile] + skip_ref[:, lanes] * state_ref[:, lanes].astype(F32)
        gate = jax.nn.sigmoid(gate_ref[:, lanes].astype(F32))
        mixed_ref[:, lanes] = (gate * jax.nn.gelu(recurrent)).astype(mixed_ref.dtype)


def spread_matrix():
    span = CHUNK * GROUP_CH
    column = np.arange(span)
    by_step = (np.arange(CHUNK)[:, None] == column[None] // GROUP_CH).astype(np.float32)
    by_channel = (np.arange(GROUP_CH)[:, None] == column[None] % GROUP_CH).astype(np.float32)
    out = np.zeros((8 * CHUNK, 4 * span), np.float32)
    for kind in range(4):
        block = by_channel if kind % 2 else by_step
        for half in range(2):
            first = (2 * kind + half) * CHUNK
            out[first : first + CHUNK, kind * span : (kind + 1) * span] = block
    return out


def shift_matrix(states2):
    span = CHUNK * GROUP_CH
    step = np.arange(CHUNK)
    upto = (step[:, None] <= (np.arange(span) // GROUP_CH)[None]).astype(np.float32)
    ref = (step < CHUNK // 2).astype(np.float32)[:, None]
    relative = upto - ref
    return np.concatenate(
        [relative, np.repeat(ref, states2, 1), np.ones((CHUNK, states2), np.float32)], axis=1
    )


def tables(decay_real, decay_frequency, log_step, chunks):
    decay_real = jnp.concatenate([decay_real, decay_real], axis=1)
    decay_frequency = jnp.concatenate([decay_frequency, decay_frequency], axis=1)
    width = decay_real.shape[1]
    low = jnp.arange(width) < width // 2
    stepsize = jnp.exp(log_step)[:, None]
    log_magnitude = decay_real * stepsize
    rotation = decay_frequency * stepsize
    magnitude = jnp.exp(log_magnitude)
    base_real = magnitude * jnp.cos(rotation)
    base_imag = magnitude * jnp.sin(rotation)
    denominator = decay_real * decay_real + decay_frequency * decay_frequency
    less_real = base_real - 1.0
    zoh_real = (less_real * decay_real + base_imag * decay_frequency) / denominator
    zoh_imag = (base_imag * decay_real - less_real * decay_frequency) / denominator
    counter = jnp.arange(1, CHUNK + 1, dtype=F32)[None, :, None]
    angle = counter * rotation[:, None, :]
    cosine, sine = jnp.cos(angle), jnp.sin(angle)
    grow = jnp.exp(counter * log_magnitude[:, None, :])
    shrink = jnp.exp(-counter * log_magnitude[:, None, :])
    power_real, power_imag = grow * cosine, grow * sine
    x1g = jnp.where(low, power_real, -power_imag)
    x3g = jnp.where(low, -power_imag, -power_real)
    x1d = shrink * cosine
    x3d = jnp.where(low, shrink * sine, -(shrink * sine))
    last_real, last_imag = power_real[:, -1], power_imag[:, -1]
    all_real, all_imag = last_real, last_imag
    for _ in range(chunks - 1):
        all_real, all_imag = (
            all_real * last_real - all_imag * last_imag,
            all_real * last_imag + all_imag * last_real,
        )
    sign = lambda value: jnp.where(low, -value, value)
    return (
        (x1g, x3g, x1d, x3d, zoh_real, sign(zoh_imag)),
        (last_real, sign(last_imag)),
        (all_real, sign(all_imag)),
    )


def on_device(
    hidden,
    query_weight,
    key_weight,
    value_weight,
    head_gate_weight,
    state_in_weight,
    state_gate_weight,
    sink_logit,
    decay_real,
    decay_frequency,
    log_step,
    input_real,
    input_imaginary,
    output_real,
    output_imaginary,
    skip_weight,
    decay_shift,
    head_out_weight,
    state_out_weight,
):
    portion = gather_hidden(hidden)
    state_input, query, key, value, head_gate, state_gate = (
        jnp.dot(portion, weight, preferred_element_type=F32).astype(BF16)
        for weight in (
            state_in_weight, query_weight, key_weight, value_weight, head_gate_weight,
            state_gate_weight,
        )
    )
    tok_rows = hidden.shape[0]
    groups, states = decay_real.shape
    chunks = tok_rows // CHUNK
    span = CHUNK * GROUP_CH
    states2 = 2 * states
    rows = groups * chunks
    prepared, (a16, b16), (a_all, b_all) = tables(decay_real, decay_frequency, log_step, chunks)
    x1g, x3g, x1d, x3d, zoh_real, zoh_imag = prepared
    sums = jnp.dot(
        decay_shift.reshape(rows, CHUNK), jnp.asarray(shift_matrix(states2)),
        precision=lax.Precision.HIGHEST,
    )
    relative = sums[:, :span]
    head = jnp.exp(sums[:, span : span + states2])
    whole_log = sums[:, span + states2 :]
    whole = jnp.exp(whole_log)
    tail = jnp.exp(whole_log - sums[:, span : span + states2])
    weight_out, weight_in = jnp.exp(relative), jnp.exp(-relative)
    tile = jnp.pad(jnp.sum(decay_shift, axis=1)[None], ((0, 7), (0, LANES - groups)))
    intra, g_out, pushed, message = pl.pallas_call(
        local_kernel,
        out_shape=(
            jax.ShapeDtypeStruct((rows, span), F32),
            jax.ShapeDtypeStruct((groups, span, states2), BF16),
            jax.ShapeDtypeStruct((rows, states2), F32),
            jax.ShapeDtypeStruct((groups + 8, LANES), F32),
        ),
        in_specs=[VMEM] * 18,
        out_specs=(VMEM,) * 4,
        scratch_shapes=[
            pltpu.VMEM((groups * GROUP_CH // LANES, tok_rows, LANES), F32),
            pltpu.VMEM((rows, span), BF16),
        ],
        compiler_params=params(),
        name="state_local",
    )(
        state_input, weight_in, x1g, x3g, x1d, x3d, input_real.transpose(0, 2, 1),
        input_imaginary.transpose(0, 2, 1), output_real, output_imaginary, zoh_real, zoh_imag,
        jnp.asarray(spread_matrix().T, BF16), a16, b16, tail, whole, tile,
    )
    count = lax.axis_size("sp")
    carry, head_mixed = pl.pallas_call(
        carry_kernel,
        out_shape=(
            jax.ShapeDtypeStruct((groups, states2), F32),
            jax.ShapeDtypeStruct(query.shape, BF16),
        ),
        in_specs=[VMEM] * 7 + [pl.BlockSpec(memory_space=pltpu.SMEM)],
        out_specs=(VMEM, VMEM),
        scratch_shapes=[
            pltpu.VMEM((count, groups + 8, LANES), F32),
            pltpu.VMEM((WINDOW + tok_rows, key.shape[1]), BF16),
            pltpu.VMEM((WINDOW + tok_rows, key.shape[1]), BF16),
            pltpu.SemaphoreType.DMA((count,)),
            pltpu.SemaphoreType.DMA((count,)),
            pltpu.SemaphoreType.DMA((2,)),
            pltpu.SemaphoreType.DMA((2,)),
        ],
        compiler_params=params(2),
        name="carry_and_attention",
    )(message, a_all, b_all, query, key, value, head_gate, sink_logit)
    state_mixed = pl.pallas_call(
        finish_kernel,
        out_shape=jax.ShapeDtypeStruct((tok_rows, groups * GROUP_CH), BF16),
        in_specs=[VMEM] * 12,
        out_specs=VMEM,
        scratch_shapes=[
            pltpu.VMEM((rows, states2), F32),
            pltpu.VMEM((rows, span), F32),
            pltpu.VMEM((groups * GROUP_CH // LANES, tok_rows, LANES), F32),
        ],
        compiler_params=params(),
        name="state_finish",
    )(
        carry, pushed, intra, g_out, weight_out, a16, b16, head, whole, state_input, state_gate,
        skip_weight.reshape(1, -1),
    )
    return project_out(head_mixed, state_mixed, head_out_weight, state_out_weight)


def solution(mesh):
    in_specs = (
        P("sp", "tp"),
        P(None, "tp"),
        P(None, "tp"),
        P(None, "tp"),
        P(None, "tp"),
        P(None, "tp"),
        P(None, "tp"),
        P("tp"),
        P("tp", None),
        P("tp", None),
        P("tp"),
        P("tp", None, None),
        P("tp", None, None),
        P("tp", None, None),
        P("tp", None, None),
        P("tp", None),
        P("tp", "sp"),
        P("tp", None),
        P("tp", None),
    )
    out_specs = P("sp", "tp")
    return jax.shard_map(
        on_device, mesh=mesh, in_specs=in_specs, out_specs=out_specs, check_vma=False
    )
```

time: 171 us -> 76.7 us (0.45)
  local copies, waits for them, and re-layouts: 75.9 us -> 8.23 us
  other arithmetic: 30.3 us -> 5.54 us
  Pallas kernels: 43.3 us -> 48.8 us
  matrix products: 16.9 us -> 13.3 us
  starting transfers between devices: 3.11 us -> 0 us
    convert_element_type x7 -> x0, local copies, waits for them, and re-layouts: 21.1 us -> none  [the longest x3 13.9 us: recur(): uw = (u.astype(F32) * jnp.exp(-relative)).astype(BF16)]
    concatenate x6 -> x0, local copies, waits for them, and re-layouts: 20 us -> none  [the longest x4 10.7 us: tables(): stack = lambda a, b: jnp.concatenate([a, b], axis=1)]
    reshape x6 -> x2, local copies, waits for them, and re-layouts: 13.1 us -> 0.78 us  [the longest x1 0.66 us: on_device(): skip_weight.reshape(1, -1)]
    convert_element_type x3 -> x0, other arithmetic: 9.77 us -> none  [halves(): return [high.astype(BF16), (value - high).astype(BF16)]]
    reduce_precision x4 -> x0, local copies, waits for them, and re-layouts: 9.73 us -> none  [halves(): high = lax.reduce_precision(value, 8, 7)]
    transpose x1 -> x0, local copies, waits for them, and re-layouts: 6.65 us -> none  [recur(): recurrent = recurrent.reshape(groups, chunks, CHUNK, GROUP_CH).transpose(...]
    pallas_call x3, Pallas kernels: 30 us -> 36.2 us  [the longest x1 15.8 us: on_device(): pl.pallas_call(carry_kernel, out_shape=(jax.ShapeDtypeStruct((groups, sta...]
    neg x4 -> x0, other arithmetic: 4.85 us -> none  [the longest x1 1.77 us: tables(): z3 = beside(-inv_imag, inv_imag)]
  transfers between devices with their start and end apart: 1 -> 0, of which waited for: 0 -> 0; matrix products, arithmetic and copies ran while one was open for 61% -> 0% of each run, Pallas kernels for 18% -> 0%
where the time goes in v2:
time: 76.7 us; the launch traced here: 76 us
  Pallas kernels  48.8 us (64%)
  matrix products  13.3 us (17%)
  local copies, waits for them, and re-layouts  8.23 us (11%)
  other arithmetic  5.54 us (7%)
    pallas_call x1, Pallas kernels, on_device(): pl.pallas_call(carry_kernel, out_shape=(jax.ShapeDtypeStruct((groups, sta...  15.8 us
    pallas_call x1, Pallas kernels, on_device(): pl.pallas_call(local_kernel, out_shape=(jax.ShapeDtypeStruct((rows, span)...  14.2 us
    dot_general x6, matrix products, on_device(): jnp.dot(portion, weight, preferred_element_type=F32).astype(BF16)  12.3 us
    pallas_call x1, Pallas kernels, project_out(): pl.pallas_call(output_kernel, out_shape=jax.ShapeDtypeStruct((rows, width...  8.4 us
    pallas_call x1, Pallas kernels, on_device(): pl.pallas_call(finish_kernel, out_shape=jax.ShapeDtypeStruct((tok_rows, g...  6.2 us
    pallas_call x1, Pallas kernels, gather_hidden(): pl.pallas_call(hidden_kernel, out_shape=jax.ShapeDtypeStruct((rows, 2 * w...  4.24 us
    select_n x2, other arithmetic, tables(): sign = lambda value: jnp.where(low, -value, value)  2.23 us
    unnamed x18, local copies, waits for them, and re-layouts  1.98 us

profile of v2, /device:TPU:29, one launch (start us, length us, event | category | flops | bytes accessed | tf_op | source)
XLA Modules:
  0.0 76.0 jit_solution(12693307690127511063)
XLA Ops:
  0.0 0.8 %exp.28 = f32[32]{0:T(128)S(1)} exponential(f32[32]{0:T(128)} %param.31) | non-fusion elementwise | bytes 256 | tf_op jit(solution)/shard_map/exp | solution.py:432
  0.8 1.6 %negate_select_fusion.5 = (f32[32,128]{1,0:T(8,128)}, f32[32,128]{1,0:T(8,128)}, f32[32,128]{1,0:T(8,128)S(1)}, f32[32,128]{1,0:T(8,128)S(1)}) fusion(f32[32,64]{1,0:T(8,128)} %param.30, f32[32,64]{1,0:T(8,128)} %param.29, pred[128]{0:T(512)(128)(4,1)S(1)} %iota_compare_fusion, f32[32]{0:T(128)S(1)} %exp.28), kind=kLoop, calls=%fused_computation.25 | loop fusion | flops 81920 | bytes 82176 | tf_op jit(solution)/shard_map/jit(_where)/select_n | solution.py:459
  2.4 1.1 %negate_select_fusion = (f32[32,16,128]{2,0,1:T(8,128)S(1)}, f32[32,16,128]{2,0,1:T(8,128)S(1)}, f32[32,16,128]{2,0,1:T(8,128)S(1)}, f32[32,16,128]{2,0,1:T(8,12...) fusion(f32[16]{0:T(128)S(1)} %get-tuple-element.36, f32[32,128]{1,0:T(8,128)S(1)} %get-tuple-element.34, ...), kind=kLoop, calls=%fused_computation.9 | loop fusion | flops 851968 | bytes 1605888 | tf_op jit(solution)/shard_map/jit(_where)/select_n | solution.py:451
  3.5 0.7 negate_select_fusion.3
  4.2 0.6 slice_bitcast_fusion.1.a16_ref
  4.8 0.9 %copy.29.x1g_ref = f32[32,16,128]{2,1,0:T(8,128)} copy(f32[32,16,128]{2,0,1:T(8,128)S(1)} %get-tuple-element.26) | data formatting | bytes 524288 | tf_op jit(solution)/shard_map/jit(_where)/select_n | solution.py:448
  5.7 0.9 %copy.30.x3g_ref = f32[32,16,128]{2,1,0:T(8,128)} copy(f32[32,16,128]{2,0,1:T(8,128)S(1)} %get-tuple-element.27) | data formatting | bytes 524288 | tf_op jit(solution)/shard_map/jit(_where)/select_n | solution.py:449
  6.5 0.9 %copy.31.x1d_ref = f32[32,16,128]{2,1,0:T(8,128)} copy(f32[32,16,128]{2,0,1:T(8,128)S(1)} %get-tuple-element.28) | data formatting | bytes 524288 | tf_op jit(solution)/shard_map/mul | solution.py:450
  7.4 0.9 %copy.32.x3d_ref = f32[32,16,128]{2,1,0:T(8,128)} copy(f32[32,16,128]{2,0,1:T(8,128)S(1)} %get-tuple-element.25) | data formatting | bytes 524288 | tf_op jit(solution)/shard_map/jit(_where)/select_n | solution.py:451
  8.3 4.2 %hidden_exchange.1 = bf16[256,2048]{1,0:T(8,128)(2,1)} custom-call(bf16[256,1024]{1,0:T(8,128)(2,1)} %own_ref.1), custom_call_target="tpu_custom_call" | custom-call | tf_op jit(solution)/shard_map/hidden_exchange/pallas_call | solution.py:52
  12.5 0.0 copy-done
  12.5 0.0 copy-start.4
  12.5 0.0 copy-start.5
  12.5 2.6 %convolution_convert_fusion.3.state_ref = bf16[256,512]{1,0:T(8,128)(2,1)} fusion(bf16[256,2048]{1,0:T(8,128)(2,1)} %hidden_exchange.1, bf16[2048,512]{1,0:T(8,128)(2,1)S(1)} %copy-done), kind=kOutput, calls=%fused_computation.4 | convolution fusion | flops 537001984 | bytes 3407872 | tf_op jit(solution)/shard_map/dot_general | solution.py:490
  15.2 0.1 reshape.64
  15.3 1.0 %convolution_bitcast_fusion = f32[512,512]{1,0:T(8,128)S(1)} fusion(f32[16,512]{1,0:T(8,128)S(1)} %copy-done.5, f32[512,16]{1,0:T(8,128)S(1)} %reshape.64), kind=kOutput, calls=%fused_computation | convolution fusion | flops 50331648 | bytes 1114112 | tf_op jit(solution)/shard_map/dot_general | solution.py:504
  16.3 1.0 %slice_exponential_fusion.1 = (f32[512,128]{1,0:T(8,128)}, f32[512,128]{1,0:T(8,128)}, f32[512,128]{1,0:T(8,128)}) fusion(f32[512,512]{1,0:T(8,128)S(1)} %convolution_bitcast_fusion), kind=kLoop, calls=%fused_computation.20 | loop fusion | flops 65536 | bytes 1310720 | tf_op jit(solution)/shard_map/exp | solution.py:509
  17.2 1.1 %slice_exponential_fusion = (f32[512,256]{1,0:T(8,128)}, f32[512,256]{1,0:T(8,128)}) fusion(f32[512,512]{1,0:T(8,128)S(1)} %convolution_bitcast_fusion), kind=kLoop, calls=%fused_computation.8 | loop fusion | flops 131072 | bytes 1572864 | tf_op jit(solution)/shard_map/exp | solution.py:513
  18.3 0.1 reduce_sum.9
  18.5 0.6 pad.4.tile_ref
  19.1 14.2 %state_local.1 = (f32[512,256]{1,0:T(8,128)}, bf16[32,256,128]{2,1,0:T(8,128)(2,1)}, f32[512,128]{1,0:T(8,128)}, f32[40,128]{1,0:T(8,128)}) custom-call(bf16[256,512]{1,0:T(8,128)(2,1)} %convolution_convert_fusion.3.state_ref, f32[512,256]{1,0:T(8,128)} %get-tuple-element.21.win_ref, f32[32,16,128]{2,1,0:T(8,128)} %copy.29.x1g_ref, ...), custom_call_target="tpu_custom_call" | custom-call | tf_op jit(solution)/shard_map/state_local/pallas_call | solution.py:515
  33.3 3.1 %convolution_convert_fusion.1.gate_ref = bf16[256,512]{1,0:T(8,128)(2,1)} fusion(bf16[256,2048]{1,0:T(8,128)(2,1)S(1)} %copy-done.1, bf16[2048,512]{1,0:T(8,128)(2,1)} %param.25), kind=kOutput, calls=%fused_computation.2 | convolution fusion | flops 537001984 | bytes 3407872 | tf_op jit(solution)/shard_map/dot_general | solution.py:490
  36.4 1.4 %convolution_convert_fusion.2.query_ref = bf16[256,512]{1,0:T(8,128)(2,1)} fusion(bf16[256,2048]{1,0:T(8,128)(2,1)S(1)} %copy-done.1, bf16[2048,512]{1,0:T(8,128)(2,1)S(1)} %copy-done.7), kind=kOutput, calls=%fused_computation.3 | convolution fusion | flops 537001984 | bytes 3407872 | tf_op jit(solution)/shard_map/dot_general | solution.py:490
  37.8 1.1 %convolution_convert_fusion.4.value_ref = bf16[256,256]{1,0:T(8,128)(2,1)} fusion(bf16[256,2048]{1,0:T(8,128)(2,1)S(1)} %copy-done.1, bf16[2048,256]{1,0:T(8,128)(2,1)S(1)} %copy-done.2), kind=kOutput, calls=%fused_computation.5 | convolution fusion | flops 268500992 | bytes 2228224 | tf_op jit(solution)/shard_map/dot_general | solution.py:490
  38.9 1.1 %convolution_convert_fusion.5.key_ref = bf16[256,256]{1,0:T(8,128)(2,1)} fusion(bf16[256,2048]{1,0:T(8,128)(2,1)S(1)} %copy-done.1, bf16[2048,256]{1,0:T(8,128)(2,1)S(1)} %copy-done.3), kind=kOutput, calls=%fused_computation.6 | convolution fusion | flops 268500992 | bytes 2228224 | tf_op jit(solution)/shard_map/dot_general | solution.py:490
  40.0 15.8 %carry_and_attention.1 = (f32[32,128]{1,0:T(8,128)}, bf16[256,512]{1,0:T(8,128)(2,1)}) custom-call(f32[40,128]{1,0:T(8,128)} %get-tuple-element.11.msg_ref, f32[32,128]{1,0:T(8,128)} %get-tuple-element.23.same_ref, f32[32,128]{1,0:T(8,128)} %get-tuple-element.22.swapped_ref, bf16[256,512]{1,0:T(8,128)(2,1)} %convolution_convert_fusion.2.query_ref, ...), custom_call_target="tpu_custom_call" | custom-call | tf_op jit(solution)/shard_map/carry_and_attention/pallas_call | solution.py:537
  55.8 3.0 %convolution_convert_fusion.gate_ref = bf16[256,512]{1,0:T(8,128)(2,1)} fusion(bf16[256,2048]{1,0:T(8,128)(2,1)S(1)} %copy-done.1, bf16[2048,512]{1,0:T(8,128)(2,1)} %param.27), kind=kOutput, calls=%fused_computation.1 | convolution fusion | flops 537001984 | bytes 3407872 | tf_op jit(solution)/shard_map/dot_general | solution.py:490
  58.8 0.1 copy.33
  58.9 0.7 reshape.65.skip_ref
  59.5 6.2 %state_finish.1.state_ref = bf16[256,512]{1,0:T(8,128)(2,1)} custom-call(f32[32,128]{1,0:T(8,128)} %get-tuple-element.13.carry_ref, f32[512,128]{1,0:T(8,128)} %get-tuple-element.14.pushed_ref, f32[512,256]{1,0:T(8,128)} %get-tuple-element.15.intra_ref, bf16[32,256,128]{2,1,0:T(8,128)(2,1)} %get-tuple-element.16.g_ref, ...), custom_call_target="tpu_custom_call" | custom-call | tf_op jit(solution)/shard_map/state_finish/pallas_call | solution.py:557
  65.7 8.4 %output_projection.1 = bf16[256,1024]{1,0:T(8,128)(2,1)} custom-call(bf16[256,512]{1,0:T(8,128)(2,1)} %get-tuple-element.12.head_ref, bf16[256,512]{1,0:T(8,128)(2,1)} %state_finish.1.state_ref, bf16[512,2048]{1,0:T(8,128)(2,1)} %how_ref.1, bf16[512,2048]{1,0:T(8,128)(2,1)} %sow_ref.1), custom_call_target="tpu_custom_call" | custom-call | tf_op jit(solution)/shard_map/output_projection/pallas_call | solution.py:106
  74.1 1.9 %copy.36 = bf16[256,1024]{1,0:T(8,128)(2,1)} copy(bf16[256,1024]{1,0:T(8,128)(2,1)} %output_projection.1) | data formatting | bytes 1048576
  (15 shorter events, 0.0 us)
Async XLA Ops:
  0.0 12.5 %copy-start = (bf16[2048,512]{1,0:T(8,128)(2,1)S(1)}, bf16[2048,512]{1,0:T(8,128)(2,1)}, u32[]{:S(2)}) copy-start(bf16[2048,512]{1,0:T(8,128)(2,1)} %param.26) | copy-start | bytes 6291460
  12.5 2.7 %copy-start.4 = (f32[32,256]{1,0:T(8,128)S(1)}, f32[32,256]{1,0:T(8,128)}, u32[]{:S(2)}) copy-start(f32[32,256]{1,0:T(8,128)} %param.37) | copy-start | bytes 98308
  12.5 2.8 %copy-start.5 = (f32[16,512]{1,0:T(8,128)S(1)}, f32[16,512]{1,0:T(8,128)}, u32[]{:S(2)}) copy-start(f32[16,512]{1,0:T(8,128)} %constant.15.clone) | copy-start | bytes 98308
  18.3 14.9 %copy-start.1 = (bf16[256,2048]{1,0:T(8,128)(2,1)S(1)}, bf16[256,2048]{1,0:T(8,128)(2,1)}, u32[]{:S(2)}) copy-start(bf16[256,2048]{1,0:T(8,128)(2,1)} %hidden_exchange.1) | copy-start | bytes 3145732
  33.3 3.2 %copy-start.7 = (bf16[2048,512]{1,0:T(8,128)(2,1)S(1)}, bf16[2048,512]{1,0:T(8,128)(2,1)}, u32[]{:S(2)}) copy-start(bf16[2048,512]{1,0:T(8,128)(2,1)} %param.22) | copy-start | bytes 6291460
  36.4 1.4 %copy-start.2 = (bf16[2048,256]{1,0:T(8,128)(2,1)S(1)}, bf16[2048,256]{1,0:T(8,128)(2,1)}, u32[]{:S(2)}) copy-start(bf16[2048,256]{1,0:T(8,128)(2,1)} %param.24) | copy-start | bytes 3145732
  36.4 2.5 %copy-start.3 = (bf16[2048,256]{1,0:T(8,128)(2,1)S(1)}, bf16[2048,256]{1,0:T(8,128)(2,1)}, u32[]{:S(2)}) copy-start(bf16[2048,256]{1,0:T(8,128)(2,1)} %param.23) | copy-start | bytes 3145732
  40.0 18.8 %copy-start.6 = (f32[32,16]{0,1:T(8,128)S(1)}, f32[32,16]{0,1:T(8,128)}, u32[]{:S(2)}) copy-start(f32[32,16]{0,1:T(8,128)} %param.36) | copy-start | bytes 6148
